TPU v7x, 32 devices: a whole 2x2x4 slice. The times are simulated.
32 devices in a mesh: sp: 8 (over z, y), tp: 4 (over x, core).
Axes of the slice: x: 2, y: 2, z: 4, core: 2. Of those that a mesh axis runs over, the one named last changes fastest.
Arguments:
- residual: bfloat16 [8192, 2048], P('sp'), may hold values from -6 to 6
- small_heads: bfloat16 [8192, 1024], P('sp', 'tp'), may hold values from -6 to 6
- large_heads: bfloat16 [8192, 1024], P('sp', 'tp'), may hold values from -6 to 6
- state_keys: bfloat16 [8192, 8, 128], P('sp', 'tp'), may hold values from -6 to 6
- state_queries: bfloat16 [8192, 8, 128], P('sp', 'tp'), may hold values from -6 to 6
- small_gate: bfloat16 [8192, 1024], P('sp', 'tp'), may hold values from -6 to 6
- large_gate: bfloat16 [8192, 1024], P('sp', 'tp'), may hold values from -6 to 6
- small_step: float32 [8192, 16], P('sp', 'tp'), may hold values from -3 to 2
- large_step: float32 [8192, 8], P('sp', 'tp'), may hold values from -3 to 2
- small_taps: bfloat16 [4, 1024], P(None, 'tp'), may hold values from -3 to 3
- large_taps: bfloat16 [4, 1024], P(None, 'tp'), may hold values from -3 to 3
- key_taps: bfloat16 [4, 8, 128], P(None, 'tp'), may hold values from -3 to 3
- query_taps: bfloat16 [4, 8, 128], P(None, 'tp'), may hold values from -3 to 3
- small_decay: float32 [16], P('tp'), may hold values from -12 to -2, as said below
- large_decay: float32 [8], P('tp'), may hold values from -12 to -2, as said below
- small_gain: bfloat16 [1024], P('tp'), may hold values from 0.099609375 to 1.8984375
- large_gain: bfloat16 [1024], P('tp'), may hold values from 0.099609375 to 1.8984375
- small_out: bfloat16 [1024, 2048], P('tp'), may hold values from -0.125 to 0.125
- large_out: bfloat16 [1024, 2048], P('tp'), may hold values from -0.125 to 0.125
- mixer_gain: bfloat16 [2048], replicated, may hold values from 0.099609375 to 1.8984375
- ffn_in_gain: bfloat16 [2048], replicated, may hold values from 0.099609375 to 1.8984375
- gate_proj: bfloat16 [2048, 5632], P('sp', 'tp'), may hold values from -0.125 to 0.125
- up_proj: bfloat16 [2048, 5632], P('sp', 'tp'), may hold values from -0.125 to 0.125
- down_proj: bfloat16 [2048, 5632], P('sp', 'tp'), may hold values from -0.078125 to 0.078125
- ffn_out_gain: bfloat16 [2048], replicated, may hold values from 0.099609375 to 1.8984375
Outputs:
- updated: bfloat16 [8192, 2048], P(('sp', 'tp'))
Inputs may be any that keep to these rules, and one draw needn't show every extreme that they name: `small_decay`: log decay rates of the first group. `large_decay`: log decay rates of the second group.
All inputs are finite; a program needn't handle non-finite values.
Results may differ from a plain program's by a relative error of at most 0.014.
Values may be sent and summed in bfloat16 or wider, within the bound.
A program may use at most 192 MiB of HBM per device.

v0:
```python
import functools

import jax
import jax.numpy as jnp
from jax import lax
from jax.experimental import pallas as pl
from jax.experimental.pallas import tpu as pltpu
from jax.sharding import PartitionSpec as P

BLOCK = 128
HALO = 16
LANES = 128
SLOTS = 8
TAIL = 16


EPS = 1e-06
OUTER, INNER = "so", "si"
SEQ = (OUTER, INNER)
CHIP, CORE = "tx", "tc"
HEADS = (CHIP, CORE)
MESH = pl.DeviceIdType.MESH
VMEM_BYTES = 64 * 1024 * 1024 - 128 * 1024
FAR = -1e30
F32 = jnp.float32
BF16 = jnp.bfloat16


def moved(block, axis, route):
    return lax.ppermute(block, axis, route)


def earlier(block, axis, distance):
    devices = range(lax.axis_size(axis))
    return moved(block, axis, [(i - distance, i) for i in devices if i - distance in devices])


def paired(block, axis, bit):
    return moved(block, axis, [(i, i ^ bit) for i in range(lax.axis_size(axis))])


def silu(x):
    return x / (1.0 + jnp.exp(-x))


def softplus(x):
    return jnp.maximum(x, 0.0) + jnp.log1p(jnp.exp(-jnp.abs(x)))


def exact_dot(a, b):
    return lax.dot_general(
        a, b, (((1,), (0,)), ((), ())), precision=lax.Precision.HIGHEST, preferred_element_type=F32
    )


def lower(n):
    rows = lax.broadcasted_iota(jnp.int32, (n, n), 0)
    return rows >= lax.broadcasted_iota(jnp.int32, (n, n), 1)


def spread(columns, heads, dim):
    rows = columns.shape[0]
    parts = []
    if dim >= LANES:
        for h in heads:
            parts.append(jnp.broadcast_to(columns[:, h : h + 1], (rows, dim)))
    else:
        per = LANES // dim
        lane = lax.broadcasted_iota(jnp.int32, (rows, LANES), 1)
        for first in range(0, len(heads), per):
            part = jnp.broadcast_to(columns[:, heads[first] : heads[first] + 1], (rows, LANES))
            for j in range(1, per):
                h = heads[first + j]
                part = jnp.where(lane >= j * dim, columns[:, h : h + 1], part)
            parts.append(part)
    return jnp.concatenate(parts, axis=1)


def conv_kernel(
    sizes, small, large, keys, queries, halo, taps, steps, decay, conv, packed, before, state, total
):
    (heads_a, dim_a), (heads_b, dim_b), state_len = sizes
    step = pl.program_id(0)

    @pl.when(step == 0)
    def _():
        before[...] = halo[...]
        state[...] = jnp.zeros_like(state)
        total[...] = jnp.zeros_like(total)

    column = 0
    for ref in (small, large, keys, queries):
        width = ref.shape[1]
        for start in range(0, width, LANES):
            here = pl.ds(column, LANES)
            now = ref[:, pl.ds(start, LANES)]
            extended = jnp.concatenate([before[:, here], now], axis=0).astype(F32)
            kernel_len = taps.shape[0]
            summed = None
            for k in range(kernel_len):
                first = HALO - kernel_len + 1 + k
                term = taps[k : k + 1, here] * extended[first : first + BLOCK]
                summed = term if summed is None else summed + term
            done = silu(summed).astype(BF16)
            conv[:, here] = done
            before[:, here] = now[BLOCK - HALO :]
            column += LANES
    dt = softplus(steps[...])
    cum = exact_dot(lower(BLOCK).astype(F32), -dt * jnp.exp(decay[...]))
    tail = cum[BLOCK - 1 : BLOCK]
    scale = dt * jnp.exp(tail - cum)
    head_list_a = list(range(heads_a))
    head_list_b = list(range(heads_a, heads_a + heads_b))
    kept = jnp.exp(tail)
    offset = 0
    width_a = heads_a * dim_a
    width_b = heads_b * dim_b
    for heads, dim, width, key_at in (
        (head_list_a, dim_a, width_a, width_a + width_b),
        (head_list_b, dim_b, width_b, width_a + width_b + state_len),
    ):
        x = conv[:, offset : offset + width].astype(F32)
        u = (x * spread(scale, heads, dim)).astype(BF16)
        k = conv[:, key_at : key_at + state_len]
        fresh = lax.dot_general(k, u, (((0,), (0,)), ((), ())), preferred_element_type=F32)
        old = state[:, offset : offset + width]
        state[:, offset : offset + width] = old * spread(kept, heads, dim) + fresh
        offset += width
    total[...] = total[...] + tail

    @pl.when(step == pl.num_programs(0) - 1)
    def _():
        packed[:state_len] = state[...].astype(BF16)
        whole = jnp.concatenate(
            [spread(total[...], head_list_a, dim_a), spread(total[...], head_list_b, dim_b)], axis=1
        )
        high = whole.astype(BF16)
        low = (whole - high.astype(F32)).astype(BF16)
        row = lax.broadcasted_iota(jnp.int32, (TAIL, whole.shape[1]), 0)
        both = jnp.where(row == 0, high.astype(F32), jnp.where(row == 1, low.astype(F32), 0.0))
        packed[state_len:] = both.astype(BF16)


def mix_kernel(
    sizes,
    place,
    conv,
    small_gate,
    large_gate,
    steps,
    steps_across,
    decay,
    decay_across,
    gain,
    small_out,
    large_out,
    entering,
    partial_out,
    state,
):
    (heads_a, dim_a), (heads_b, dim_b), state_len = sizes
    step = pl.program_id(0)

    @pl.when(step == 0)
    def _():
        state[...] = entering[...]

    causal = lower(BLOCK)
    ones = causal.astype(F32)
    dt = softplus(steps[...])
    cum = exact_dot(ones, -dt * jnp.exp(decay[...]))
    dt_across = softplus(steps_across[...])
    upper = (
        lax.broadcasted_iota(jnp.int32, (BLOCK, BLOCK), 0)
        <= lax.broadcasted_iota(jnp.int32, (BLOCK, BLOCK), 1)
    ).astype(F32)
    cum_across = exact_dot(-dt_across * jnp.exp(decay_across[...]), upper)
    tail = cum[BLOCK - 1 : BLOCK]
    scale = dt * jnp.exp(tail - cum)
    grown = jnp.exp(cum)
    kept = jnp.exp(tail)
    width_a = heads_a * dim_a
    width_b = heads_b * dim_b
    offset = 0
    result = None
    lane = lax.broadcasted_iota(jnp.int32, (BLOCK, LANES), 1)
    for which, (heads, dim, width, gate, out) in enumerate(
        (
            (list(range(heads_a)), dim_a, width_a, small_gate, small_out),
            (list(range(heads_a, heads_a + heads_b)), dim_b, width_b, large_gate, large_out),
        )
    ):
        key_at = width_a + width_b + which * state_len
        query_at = key_at + 2 * state_len
        x = conv[:, offset : offset + width]
        k = conv[:, key_at : key_at + state_len]
        q = conv[:, query_at : query_at + state_len]
        scores = lax.dot_general(q, k, (((1,), (1,)), ((), ())), preferred_element_type=F32)
        old = state[:, offset : offset + width]
        carried = jnp.dot(q, old.astype(BF16), preferred_element_type=F32)
        carried = carried * spread(grown, heads, dim)
        u = (x.astype(F32) * spread(scale, heads, dim)).astype(BF16)
        fresh = lax.dot_general(k, u, (((0,), (0,)), ((), ())), preferred_element_type=F32)
        state[:, offset : offset + width] = old * spread(kept, heads, dim) + fresh
        inside = []
        span = max(dim, LANES)
        per = span // dim
        for first in range(0, len(heads), per):
            x_part = x[:, first * dim : first * dim + span]
            part = None
            for j in range(per):
                h = heads[first + j]
                gap = cum[:, h : h + 1] - cum_across[h : h + 1]
                decays = jnp.exp(jnp.where(causal, gap, FAR))
                w = (scores * decays * dt_across[h : h + 1]).astype(BF16)
                got = jnp.dot(w, x_part, preferred_element_type=F32)
                part = got if part is None else jnp.where(lane >= j * dim, got, part)
            inside.append(part)
        mixed = jnp.concatenate(inside, axis=1) + carried
        gated = mixed * silu(gate[...].astype(F32))
        squares = gated * gated
        normed = []
        for first in range(0, len(heads), per):
            at = first * dim
            part = squares[:, at : at + span]
            means = None
            for j in range(per):
                if per == 1:
                    means = jnp.sum(part, axis=1, keepdims=True)
                else:
                    ours = (lane >= j * dim) & (lane < (j + 1) * dim)
                    one = jnp.sum(jnp.where(ours, part, 0.0), axis=1, keepdims=True)
                    means = one if means is None else jnp.where(lane >= j * dim, one, means)
            normed.append(gated[:, at : at + span] * lax.rsqrt(means * (1.0 / dim) + EPS))
        normed = jnp.concatenate(normed, axis=1) * gain[:, offset : offset + width]
        product = jnp.dot(normed.astype(BF16), out[...], preferred_element_type=F32)
        result = product if result is None else result + product
        offset += width
    partial_out[...] = result.astype(BF16)[None]


def unit_rms(values):
    return values * lax.rsqrt(jnp.mean(values * values, axis=-1, keepdims=True) + EPS)


def norm_kernel(one, other, own, mixer_gain, ffn_gain, mixed_out, normed_out):
    mix = one[...].astype(F32) + other[...].astype(F32)
    mixed = own[...].astype(F32) + unit_rms(mix) * mixer_gain[...].astype(F32)
    mixed_out[...] = mixed
    normed_out[...] = (unit_rms(mixed) * ffn_gain[...].astype(F32)).astype(BF16)


def half_width(columns):
    return (columns // LANES + 1) // 2 * LANES


def greet(partners):
    barrier = pltpu.get_barrier_semaphore()
    for partner in partners:
        pl.semaphore_signal(barrier, inc=1, device_id=partner, device_id_type=MESH)
    pl.semaphore_wait(barrier, len(partners))


def remote(source, target, send, recv, partner):
    copy = pltpu.make_async_remote_copy(
        src_ref=source,
        dst_ref=target,
        send_sem=send,
        recv_sem=recv,
        device_id=partner,
        device_id_type=MESH,
    )
    return copy


def weights_kernel(count, sources, targets, sems):
    send, recv, side_send, side_recv, local_sem = sems
    z, y = lax.axis_index(OUTER), lax.axis_index(INNER)
    rows, columns = sources[0].shape
    wide = targets[0].shape[1]
    partner = {INNER: 1 - y}
    others = {d: (z + d) % count for d in range(1, count)}
    greet([partner] + [{OUTER: other} for other in others.values()])

    def half(ref, member):
        start = pl.multiple_of(member % 2 * (columns - wide), LANES)
        return ref.at[:, pl.ds(start, wide)]

    def block(ref, index):
        return ref.at[pl.ds(pl.multiple_of((index * 2 + y) * rows, rows), rows)]

    order = sorted(others, key=lambda d: (min(d, count - d), d))
    sent, passed, kept = [], [], []
    for m, (source, target) in enumerate(zip(sources, targets)):
        for d in order:
            copy = remote(
                half(source, others[d]), block(target, z), send.at[m, d], recv.at[m, d], {OUTER: others[d]}
            )
            copy.start()
            sent.append(copy)
        copy = remote(half(source, z), block(target, z), side_send.at[m, 0], side_recv.at[m, 0], partner)
        copy.start()
        passed.append(copy)
        copy = pltpu.make_async_copy(half(source, z), block(target, z), local_sem.at[m])
        copy.start()
        kept.append(copy)
    for m, target in enumerate(targets):
        for d in order:
            here = block(target, (z + count - d) % count)
            remote(here, here, send.at[m, d], recv.at[m, d], partner).wait_recv()
            copy = remote(here, here, side_send.at[m, d], side_recv.at[m, d], partner)
            copy.start()
            passed.append(copy)
    for copy in kept:
        copy.wait()
    for copy in sent:
        copy.wait_send()
    for copy in passed:
        copy.wait()


def gather_weights_kernel(count, gate, up, down, gate_out, up_out, down_out, *sems):
    weights_kernel(count, (gate, up, down), (gate_out, up_out, down_out), sems)


def gathered(*shards):
    rows, columns = shards[0].shape
    count = lax.axis_size(OUTER)
    wide = half_width(columns)
    n = len(shards)
    return pl.pallas_call(
        functools.partial(gather_weights_kernel, count),
        in_specs=[pl.BlockSpec(memory_space=pl.ANY)] * n,
        out_specs=[pl.BlockSpec(memory_space=pltpu.VMEM)] * n,
        out_shape=[jax.ShapeDtypeStruct((2 * count * rows, wide), BF16)] * n,
        scratch_shapes=[pltpu.SemaphoreType.DMA((n, count))] * 4 + [pltpu.SemaphoreType.DMA((n,))],
        compiler_params=pltpu.CompilerParams(
            collective_id=0, has_side_effects=True, vmem_limit_bytes=VMEM_BYTES
        ),
        cost_estimate=pl.CostEstimate(flops=1_000_000_000, bytes_accessed=rows, transcendentals=0),
        name="weights",
    )(*shards)


def ffn_kernel(
    overlap,
    normed,
    gate_weights,
    up_weights,
    down_weights,
    mixed,
    gain,
    out,
    blocks,
    local,
    to_core,
    from_core,
    hop,
    got,
    send,
    recv,
    core_send,
    core_recv,
    hop_send,
    hop_recv,
):
    z, x, c = lax.axis_index(OUTER), lax.axis_index(CHIP), lax.axis_index(CORE)
    pair = z % 2

    def flipped(value, by):
        return value + by * (1 - 2 * value)

    def place(core, d_one, d_two):
        dz = d_one * (1 - core) + d_two * core
        dx = d_one * core + d_two * (1 - core)
        return (flipped(pair, dz) * 2 + flipped(x, dx)) * 2 + core

    near = {CORE: 1 - c}
    one = {OUTER: z + (1 - c) * (1 - 2 * pair), CHIP: flipped(x, c)}
    two = {OUTER: z + c * (1 - 2 * pair), CHIP: flipped(x, 1 - c)}
    greet([near, one, two])
    mine = place(c, 0, 0)
    starts = []
    for index, partner in enumerate((one, two, near)):
        copy = remote(normed, blocks.at[mine], send.at[index], recv.at[mine], partner)
        copy.start()
        starts.append(copy)
    blocks[mine] = normed[...]

    def passing(slot, index, partner):
        return remote(blocks.at[slot], blocks.at[slot], send.at[index], recv.at[slot], partner)

    def product(slot):
        rows = blocks[slot]
        gate = jnp.dot(rows, gate_weights[...], preferred_element_type=F32)
        up = jnp.dot(rows, up_weights[...], preferred_element_type=F32)
        hidden = silu(gate) * up
        column = lax.broadcasted_iota(jnp.int32, hidden.shape, 1)
        hidden = jnp.where(column >= pair * overlap, hidden, 0.0).astype(BF16)
        return lax.dot_general(
            hidden, down_weights[...], (((1,), (1,)), ((), ())), preferred_element_type=F32
        )

    def to_near(j):
        return remote(to_core.at[j], from_core.at[j], core_send.at[j], core_recv.at[j], near)

    def step(j, _):
        d_one, d_two = j % 2, j // 2
        slot = place(c, d_one, d_two)

        @pl.when(j > 0)
        def _():
            passing(slot, 0, near).wait_recv()
            passing(slot, 3 + j, near).start()

        @pl.when(j == 1)
        def _():
            passing(slot, 3, two).start()

        local[j] = product(slot)
        slot = place(1 - c, d_one, d_two)
        passing(slot, 0, near).wait_recv()
        to_core[j] = product(slot).astype(BF16)
        to_near(j).start()
        return 0

    lax.fori_loop(0, 4, step, 0)

    def hopping(index, partner):
        return remote(hop.at[index], got.at[index], hop_send.at[index], hop_recv.at[index], partner)

    def chip_sum(j):
        to_near(j).wait_recv()
        return local[j] + from_core[j].astype(F32)

    hop[0] = chip_sum(3).astype(BF16)
    hopping(0, two).start()
    hop[1] = chip_sum(2).astype(BF16)
    hopping(1, two).start()
    partial = chip_sum(1)
    hopping(0, two).wait_recv()
    hop[2] = (partial + got[0].astype(F32)).astype(BF16)
    hopping(2, one).start()
    total = chip_sum(0)
    hopping(1, two).wait_recv()
    total = total + got[1].astype(F32)
    hopping(2, one).wait_recv()
    total = total + got[2].astype(F32)
    out[...] = (mixed[...] + 0.5 * unit_rms(total) * gain[...].astype(F32)).astype(BF16)
    for copy in starts:
        copy.wait_send()
    passing(mine, 3, two).wait_send()
    for j in range(4):
        to_near(j).wait_send()
        if j > 0:
            passing(mine, 3 + j, near).wait_send()
    for index, partner in enumerate((two, two, one)):
        hopping(index, partner).wait_send()


def channel_mixer(normed, weights, mixed, gain, overlap):
    share, features = normed.shape
    vmem = pl.BlockSpec(memory_space=pltpu.VMEM)
    block = (share, features)
    return pl.pallas_call(
        functools.partial(ffn_kernel, overlap),
        in_specs=[vmem] * 6,
        out_specs=vmem,
        out_shape=jax.ShapeDtypeStruct(block, BF16),
        scratch_shapes=[
            pltpu.VMEM((8, *block), BF16),
            pltpu.VMEM((4, *block), F32),
            pltpu.VMEM((4, *block), BF16),
            pltpu.VMEM((4, *block), BF16),
            pltpu.VMEM((3, *block), BF16),
            pltpu.VMEM((3, *block), BF16),
            pltpu.SemaphoreType.DMA((7,)),
            pltpu.SemaphoreType.DMA((8,)),
            pltpu.SemaphoreType.DMA((4,)),
            pltpu.SemaphoreType.DMA((4,)),
            pltpu.SemaphoreType.DMA((3,)),
            pltpu.SemaphoreType.DMA((3,)),
        ],
        compiler_params=pltpu.CompilerParams(
            collective_id=1, has_side_effects=True, vmem_limit_bytes=VMEM_BYTES
        ),
        cost_estimate=pl.CostEstimate(
            flops=40_000_000_000, bytes_accessed=share * features, transcendentals=0
        ),
        name="channel_mixer",
    )(normed, *weights, mixed, gain)


def reversed_bits(value, count):
    out = 0
    bit = 1
    while bit < count:
        out = out * 2 + (value // bit) % 2
        bit *= 2
    return out


def scattered(blocks, axis):
    bit = 1
    while True:
        half = blocks.shape[0] // 2
        other = paired(blocks[half:], axis, bit)
        if half == 1:
            return blocks[0], other[0]
        blocks = (blocks[:half].astype(F32) + other.astype(F32)).astype(BF16)
        bit *= 2


def layer(
    residual,
    small_heads,
    large_heads,
    state_keys,
    state_queries,
    small_gate,
    large_gate,
    small_step,
    large_step,
    small_taps,
    large_taps,
    key_taps,
    query_taps,
    small_decay,
    large_decay,
    small_gain,
    large_gain,
    small_out,
    large_out,
    mixer_gain,
    ffn_in_gain,
    gate_proj,
    up_proj,
    down_proj,
    ffn_out_gain,
):
    length, features = residual.shape
    state_len = state_keys.shape[-1]
    key_rows = state_keys.reshape(length, -1)
    query_rows = state_queries.reshape(length, -1)
    halo_rows = small_taps.shape[0] - 1
    first_row = length - halo_rows
    last = jnp.concatenate(
        [a[first_row:] for a in (small_heads, large_heads, key_rows, query_rows)], axis=1
    )
    halo = earlier(last, SEQ, 1)
    halo = jnp.pad(halo, ((HALO - halo_rows, 0), (0, 0)))
    weights = gathered(gate_proj, up_proj, down_proj)

    heads_a = small_step.shape[1]
    heads_b = large_step.shape[1]
    heads = heads_a + heads_b
    width_a = small_heads.shape[1]
    width_b = large_heads.shape[1]
    width = width_a + width_b
    everything = width + key_rows.shape[1] + query_rows.shape[1]
    sizes = ((heads_a, width_a // heads_a), (heads_b, width_b // heads_b), state_len)
    steps = jnp.pad(
        jnp.concatenate([small_step, large_step], axis=1), ((0, 0), (0, SLOTS - heads))
    )
    steps_across = steps.T
    decay = jnp.pad(jnp.concatenate([small_decay, large_decay]), (0, SLOTS - heads))
    taps = jnp.concatenate(
        [
            small_taps,
            large_taps,
            key_taps.reshape(halo_rows + 1, -1),
            query_taps.reshape(halo_rows + 1, -1),
        ],
        axis=1,
    ).astype(F32)
    gain = jnp.concatenate([small_gain, large_gain]).astype(F32)[None]
    blocks = length // BLOCK

    def rows(columns):
        return pl.BlockSpec((BLOCK, columns), lambda i, *_: (i, 0))

    def whole(*shape):
        return pl.BlockSpec(shape, lambda i, *_: (0,) * len(shape))

    conv, packed = pl.pallas_call(
        functools.partial(conv_kernel, sizes),
        grid=(blocks,),
        in_specs=[
            rows(width_a),
            rows(width_b),
            rows(key_rows.shape[1]),
            rows(query_rows.shape[1]),
            whole(HALO, everything),
            whole(halo_rows + 1, everything),
            rows(SLOTS),
            whole(1, SLOTS),
        ],
        out_specs=[rows(everything), whole(state_len + TAIL, width)],
        out_shape=[
            jax.ShapeDtypeStruct((length, everything), BF16),
            jax.ShapeDtypeStruct((state_len + TAIL, width), BF16),
        ],
        scratch_shapes=[
            pltpu.VMEM((HALO, everything), BF16),
            pltpu.VMEM((state_len, width), F32),
            pltpu.VMEM((1, SLOTS), F32),
        ],
        cost_estimate=pl.CostEstimate(
            flops=10_000_000_000, bytes_accessed=length * everything * 4, transcendentals=0
        ),
        name="convolve",
    )(small_heads, large_heads, key_rows, query_rows, halo, taps, steps, decay[None])

    def opened(array):
        whole_log = array[state_len : state_len + 1].astype(F32)
        whole_log = whole_log + array[state_len + 1 : state_len + 2].astype(F32)
        return array[:state_len].astype(F32), whole_log

    count = lax.axis_size(SEQ)
    near = 1
    while near * near < count:
        near *= 2
    received = [opened(earlier(packed, SEQ, d)) for d in range(1, near + 1)]
    entering, log = received[-1]
    for nearer, nearer_log in received[-2::-1]:
        entering = entering * jnp.exp(nearer_log) + nearer
        log = log + nearer_log
    distance = near
    while distance < count:
        high = lax.reduce_precision(log, 8, 7)
        sent = jnp.concatenate(
            [
                entering.astype(BF16),
                high.astype(BF16),
                (log - high).astype(BF16),
            ],
            axis=0,
        )
        far_state, far_log = opened(earlier(sent, SEQ, distance))
        entering = far_state * jnp.exp(log) + entering
        log = log + far_log
        distance *= 2

    share_count = lax.axis_size(HEADS)
    me = lax.axis_index(HEADS)
    share = length // share_count
    per_share = share // BLOCK

    def out_place(i, place):
        return (reversed_bits((i // per_share) ^ place[0], share_count), i % per_share, 0)

    partial_value = pl.pallas_call(
        functools.partial(mix_kernel, sizes),
        grid_spec=pltpu.PrefetchScalarGridSpec(
            num_scalar_prefetch=1,
            grid=(blocks,),
            in_specs=[
                rows(everything),
                rows(width_a),
                rows(width_b),
                rows(SLOTS),
                pl.BlockSpec((SLOTS, BLOCK), lambda i, *_: (0, i)),
                whole(1, SLOTS),
                whole(SLOTS, 1),
                whole(1, width),
                whole(width_a, features),
                whole(width_b, features),
                whole(state_len, width),
            ],
            out_specs=pl.BlockSpec((1, BLOCK, features), out_place),
            scratch_shapes=[pltpu.VMEM((state_len, width), F32)],
        ),
        out_shape=jax.ShapeDtypeStruct((share_count, share, features), BF16),
        cost_estimate=pl.CostEstimate(
            flops=10_000_000_000, bytes_accessed=length * features * 4, transcendentals=0
        ),
        name="mix",
    )(
        jnp.reshape(me, (1,)).astype(jnp.int32),
        conv,
        small_gate,
        large_gate,
        steps,
        steps_across,
        decay[None],
        decay[:, None],
        gain,
        small_out,
        large_out,
        entering,
    )
    mix_one, mix_other = scattered(partial_value, HEADS)
    own = lax.dynamic_slice_in_dim(residual, me * share, share, 0)
    tile = BLOCK // 2

    def strips(columns):
        return pl.BlockSpec((tile, columns), lambda i, *_: (i, 0))

    mixed, normed_own = pl.pallas_call(
        norm_kernel,
        grid=(share // tile,),
        in_specs=[strips(features)] * 3 + [whole(1, features)] * 2,
        out_specs=[strips(features)] * 2,
        out_shape=[
            jax.ShapeDtypeStruct((share, features), F32),
            jax.ShapeDtypeStruct((share, features), BF16),
        ],
        cost_estimate=pl.CostEstimate(
            flops=1_000_000_000, bytes_accessed=share * features * 12, transcendentals=0
        ),
        name="norms",
    )(mix_one, mix_other, own, mixer_gain[None], ffn_in_gain[None])
    columns = gate_proj.shape[1]
    overlap = 2 * half_width(columns) - columns
    return channel_mixer(normed_own, weights, mixed, ffn_out_gain[None], overlap)


def solution(mesh):
    placed = (
        P(SEQ, None),
        P(SEQ, HEADS),
        P(SEQ, HEADS),
        P(SEQ, HEADS, None),
        P(SEQ, HEADS, None),
        P(SEQ, HEADS),
        P(SEQ, HEADS),
        P(SEQ, HEADS),
        P(SEQ, HEADS),
        P(None, HEADS),
        P(None, HEADS),
        P(None, HEADS, None),
        P(None, HEADS, None),
        P(HEADS),
        P(HEADS),
        P(HEADS),
        P(HEADS),
        P(HEADS, None),
        P(HEADS, None),
        P(),
        P(),
        P(SEQ, HEADS),
        P(SEQ, HEADS),
        P(SEQ, HEADS),
        P(),
    )
    outer, heads = mesh.shape["sp"] // 2, mesh.shape["tp"] // 2
    cut = jax.sharding.Mesh(mesh.devices.reshape(outer, 2, heads, 2), (OUTER, INNER, CHIP, CORE))
    return jax.shard_map(
        layer, mesh=cut, in_specs=placed, out_specs=P((*SEQ, *HEADS), None), check_vma=False
    )
```

profile of v0, /device:TPU:24, one launch (start us, length us, event | category | flops | bytes accessed | tf_op | source)
XLA Modules:
  0.0 310.2 jit_solution(1993284186203688645)
XLA Ops:
  0.0 0.7 slice_bitcast_fusion.2
  0.7 0.7 slice_bitcast_fusion.1
  1.4 0.7 slice.69
  2.1 0.7 slice.70
  2.8 3.4 %collective-permute-start = (bf16[3,1024]{1,0:T(4,128)(2,1)S(1)}, bf16[3,1024]{1,0:T(4,128)(2,1)S(1)}, u32[]{:S(2)}, u32[]{:S(2)}) collective-permute-start(bf16[3,1024]{1,0:T(4,128)(2,1)S(1)} %pad_maximum_fusion.1), channel_id=1, source_target_pairs={{0,4},{4,8},{8,12},{12,16},{16,20},{20,24},{24,28},{1,5},{5,9},{9,... | collective-permute-start | bytes 18440 | tf_op jit(solution)/shard_map/ppermute | solution.py:30
  6.2 0.7 copy_bitcast_fusion.2
  6.9 1.3 fusion.12
  8.3 2.3 copy_bitcast_fusion
  10.6 1.3 maximum_convert_fusion.taps
  11.9 1.3 fusion.18.decay
  13.2 1.0 copy.26.steps
  14.2 0.0 collective-permute-done
  14.2 0.6 pad.12.halo
  14.8 10.8 %convolve.1 = (bf16[1024,1024]{1,0:T(8,128)(2,1)}, bf16[144,512]{1,0:T(8,128)(2,1)}) custom-call(bf16[1024,256]{1,0:T(8,128)(2,1)} %small.1, bf16[1024,256]{1,0:T(8,128)(2,1)} %large.1, bf16[1024,256]{1,0:T(8,128)(2,1)} %get-tuple-element.35.keys, bf16[1024,256]{1,0:T(8,128)(2,1)} %get-tuple-element.34.queries, bf16[16,1024]{1,0:T(8,128)(2,1)} %pad.12.halo, ...), custom_call_target="tpu_custom_call" | custom-call | flops 10000000000 | bytes 4194304 | tf_op jit(solution)/shard_map/convolve/pallas_call | solution.py:585
  25.6 1.9 collective-permute-start.4
  27.5 1.3 collective-permute-start.3
  28.8 1.3 collective-permute-start.2
  30.1 1.3 collective-permute-start.1
  31.4 3.7 %collective-permute-done.4 = bf16[144,512]{1,0:T(8,128)(2,1)S(1)} collective-permute-done((bf16[144,512]{1,0:T(8,128)(2,1)}, bf16[144,512]{1,0:T(8,128)(2,1)S(1)}, u32[]{:S(2)}, u32[]{:S(2)}) %collective-permute-start.4) | collective-permute-done | bytes 147488 | tf_op jit(solution)/shard_map/ppermute | solution.py:30
  35.1 1.0 collective-permute-done.3
  36.2 13.3 %collective-permute-done.2 = bf16[144,512]{1,0:T(8,128)(2,1)S(1)} collective-permute-done((bf16[144,512]{1,0:T(8,128)(2,1)}, bf16[144,512]{1,0:T(8,128)(2,1)S(1)}, u32[]{:S(2)}, u32[]{:S(2)}) %collective-permute-start.2) | collective-permute-done | bytes 147488 | tf_op jit(solution)/shard_map/ppermute | solution.py:30
  49.5 0.0 collective-permute-done.1
  49.5 0.1 fusion.13
  49.6 1.3 collective-permute-start.5
  50.9 0.1 fusion.17
  51.0 0.7 copy.28.decay_across
  51.7 0.6 maximum_convert_fusion.1.gain
  52.3 5.2 %collective-permute-done.5 = bf16[130,512]{1,0:T(8,128)(2,1)S(1)} collective-permute-done((bf16[130,512]{1,0:T(8,128)(2,1)S(1)}, bf16[130,512]{1,0:T(8,128)(2,1)S(1)}, u32[]{:S(2)}, u32[]{:S(2)}) %collective-permute-start.5) | collective-permute-done | bytes 133152 | tf_op jit(solution)/shard_map/ppermute | solution.py:30
  57.5 0.8 multiply_add_fusion.entering
  58.3 14.4 %mix.1 = bf16[4,256,2048]{2,1,0:T(8,128)(2,1)} custom-call(s32[1]{0:T(128)} %bitcast.place, bf16[1024,1024]{1,0:T(8,128)(2,1)} %get-tuple-element.12.conv, bf16[1024,256]{1,0:T(8,128)(2,1)} %small_gate.1, bf16[1024,256]{1,0:T(8,128)(2,1)} %large_gate.1, f32[1024,8]{1,0:T(8,128)} %copy.26.steps, f32[8,1024]{1,0:T(8,128)} %get-tuple-element.26.steps_across, ...), custom_call_target="tpu_custom_call" | custom-call | flops 10000000000 | bytes 8388608 | tf_op jit(solution)/shard_map/mix/pallas_call | solution.py:652
  72.7 1.9 slice.106
  74.6 0.1 collective-permute-start.6
  74.7 4.1 %collective-permute-done.6 = bf16[2,256,2048]{2,1,0:T(8,128)(2,1)S(1)} collective-permute-done((bf16[2,256,2048]{2,1,0:T(8,128)(2,1)S(1)}, bf16[2,256,2048]{2,1,0:T(8,128)(2,1)S(1)}, u32[]{:S(2)}, u32[]{:S(2)}) %collective-permute-start.6) | collective-permute-done | bytes 2097184 | tf_op jit(solution)/shard_map/ppermute | solution.py:30
  78.8 0.9 add_convert_fusion
  79.7 0.0 copy-start.1
  79.7 0.0 copy-start.2
  79.8 0.0 copy-start.3
  79.8 1.5 fusion.16
  81.2 1.5 collective-permute-start.7
  82.7 0.6 broadcast_in_dim.19.mixer_gain
  83.4 0.6 broadcast_in_dim.20.ffn_gain
  84.0 0.6 broadcast_in_dim.21.gain
  84.6 127.9 %weights.1 = (bf16[2048,768]{1,0:T(8,128)(2,1)}, bf16[2048,768]{1,0:T(8,128)(2,1)}, bf16[2048,768]{1,0:T(8,128)(2,1)}) custom-call(bf16[256,1408]{1,0:T(8,128)(2,1)} %gate.1, bf16[256,1408]{1,0:T(8,128)(2,1)} %up.1, bf16[256,1408]{1,0:T(8,128)(2,1)} %down.1), custom_call_target="tpu_custom_call" | custom-call | flops 1000000000 | bytes 256 | tf_op jit(solution)/shard_map/weights/pallas_call | solution.py:331
  212.4 2.3 constant_dynamic-slice_fusion.own
  214.8 0.0 collective-permute-done.7
  214.8 4.5 %norms.1 = (f32[256,2048]{1,0:T(8,128)}, bf16[256,2048]{1,0:T(8,128)(2,1)}) custom-call(bf16[256,2048]{1,0:T(8,128)(2,1)} %get-tuple-element.22.one, bf16[256,2048]{1,0:T(8,128)(2,1)} %bitcast.9.other, bf16[256,2048]{1,0:T(8,128)(2,1)} %constant_dynamic-slice_fusion.own, bf16[1,2048]{1,0:T(2,128)(2,1)} %broadcast_in_dim.19.mixer_gain, ...), custom_call_target="tpu_custom_call" | custom-call | flops 1000000000 | bytes 6291456 | tf_op jit(solution)/shard_map/norms/pallas_call | solution.py:699
  219.3 88.7 %channel_mixer.1 = bf16[256,2048]{1,0:T(8,128)(2,1)} custom-call(bf16[256,2048]{1,0:T(8,128)(2,1)} %get-tuple-element.14.normed, bf16[2048,768]{1,0:T(8,128)(2,1)} %get-tuple-element.15.gate_weights, bf16[2048,768]{1,0:T(8,128)(2,1)} %get-tuple-element.16.up_weights, bf16[2048,768]{1,0:T(8,128)(2,1)} %get-tuple-element.17.down_weights, ...), custom_call_target="tpu_custom_call" | custom-call | flops 40000000000 | bytes 524288 | tf_op jit(solution)/shard_map/channel_mixer/pallas_call | solution.py:465
  307.9 2.3 copy.42
  (20 shorter events, 0.1 us)
Async XLA Ops:
  2.8 11.4 %collective-permute-start = (bf16[3,1024]{1,0:T(4,128)(2,1)S(1)}, bf16[3,1024]{1,0:T(4,128)(2,1)S(1)}, u32[]{:S(2)}, u32[]{:S(2)}) collective-permute-start(bf16[3,1024]{1,0:T(4,128)(2,1)S(1)} %pad_maximum_fusion.1), channel_id=1, source_target_pairs={{0,4},{4,8},{8,12},{12,16},{16,20},{20,24},{24,28},{1,5},{5,9},{9,... | collective-permute-start | bytes 18440 | tf_op jit(solution)/shard_map/ppermute | solution.py:30
  14.8 36.1 %copy-start.4 = (f32[2]{0:T(128)S(1)}, f32[2]{0:T(128)}, u32[]{:S(2)}) copy-start(f32[2]{0:T(128)} %param.39) | copy-start | bytes 28
  14.8 36.1 %copy-start.5 = (f32[4]{0:T(128)S(1)}, f32[4]{0:T(128)}, u32[]{:S(2)}) copy-start(f32[4]{0:T(128)} %param.38) | copy-start | bytes 52
  14.8 36.2 %copy-start.6 = (bf16[256]{0:T(256)(128)(2,1)S(1)}, bf16[256]{0:T(256)(128)(2,1)}, u32[]{:S(2)}) copy-start(bf16[256]{0:T(256)(128)(2,1)} %param.40) | copy-start | bytes 1540
  14.8 36.2 %copy-start.7 = (bf16[256]{0:T(256)(128)(2,1)S(1)}, bf16[256]{0:T(256)(128)(2,1)}, u32[]{:S(2)}) copy-start(bf16[256]{0:T(256)(128)(2,1)} %param.41) | copy-start | bytes 1540
  25.6 9.5 %collective-permute-start.4 = (bf16[144,512]{1,0:T(8,128)(2,1)}, bf16[144,512]{1,0:T(8,128)(2,1)S(1)}, u32[]{:S(2)}, u32[]{:S(2)}) collective-permute-start(bf16[144,512]{1,0:T(8,128)(2,1)} %get-tuple-element.13), channel_id=1, source_target_pairs={{0,4},{4,8},{8,12},{12,16},{16,20},{20,24},{24,28},{1,5},{5,9},{9,... | collective-permute-start | bytes 442376 | tf_op jit(solution)/shard_map/ppermute | solution.py:30
  27.5 8.6 %collective-permute-start.3 = (bf16[144,512]{1,0:T(8,128)(2,1)}, bf16[144,512]{1,0:T(8,128)(2,1)S(1)}, u32[]{:S(2)}, u32[]{:S(2)}) collective-permute-start(bf16[144,512]{1,0:T(8,128)(2,1)} %get-tuple-element.13), channel_id=1, source_target_pairs={{0,8},{4,12},{8,16},{12,20},{16,24},{20,28},{1,9},{5,13},{9,17},{1... | collective-permute-start | bytes 442376 | tf_op jit(solution)/shard_map/ppermute | solution.py:30
  28.8 20.6 %collective-permute-start.2 = (bf16[144,512]{1,0:T(8,128)(2,1)}, bf16[144,512]{1,0:T(8,128)(2,1)S(1)}, u32[]{:S(2)}, u32[]{:S(2)}) collective-permute-start(bf16[144,512]{1,0:T(8,128)(2,1)} %get-tuple-element.13), channel_id=1, source_target_pairs={{0,12},{4,16},{8,20},{12,24},{16,28},{1,13},{5,17},{9,21},{13,25},... | collective-permute-start | bytes 442376 | tf_op jit(solution)/shard_map/ppermute | solution.py:30
  30.1 19.3 %collective-permute-start.1 = (bf16[144,512]{1,0:T(8,128)(2,1)}, bf16[144,512]{1,0:T(8,128)(2,1)S(1)}, u32[]{:S(2)}, u32[]{:S(2)}) collective-permute-start(bf16[144,512]{1,0:T(8,128)(2,1)} %get-tuple-element.13), channel_id=1, source_target_pairs={{0,16},{4,20},{8,24},{12,28},{1,17},{5,21},{9,25},{13,29},{2,18},{... | collective-permute-start | bytes 442376 | tf_op jit(solution)/shard_map/ppermute | solution.py:30
  49.6 7.8 %collective-permute-start.5 = (bf16[130,512]{1,0:T(8,128)(2,1)S(1)}, bf16[130,512]{1,0:T(8,128)(2,1)S(1)}, u32[]{:S(2)}, u32[]{:S(2)}) collective-permute-start(bf16[130,512]{1,0:T(8,128)(2,1)S(1)} %pad_maximum_fusion), channel_id=1, source_target_pairs={{0,16},{4,20},{8,24},{12,28},{1,17},{5,21},{9,25},{13,29},{2,18},{... | collective-permute-start | bytes 399368 | tf_op jit(solution)/shard_map/ppermute | solution.py:30
  72.7 6.1 %copy-start = (bf16[4,256,2048]{2,1,0:T(8,128)(2,1)S(1)}, bf16[4,256,2048]{2,1,0:T(8,128)(2,1)}, u32[]{:S(2)}) copy-start(bf16[4,256,2048]{2,1,0:T(8,128)(2,1)} %mix.1) | copy-start | bytes 12582916
  74.6 4.2 %collective-permute-start.6 = (bf16[2,256,2048]{2,1,0:T(8,128)(2,1)S(1)}, bf16[2,256,2048]{2,1,0:T(8,128)(2,1)S(1)}, u32[]{:S(2)}, u32[]{:S(2)}) collective-permute-start(bf16[2,256,2048]{2,1,0:T(8,128)(2,1)S(1)} %slice.106), channel_id=1, source_target_pairs={{0,1},{1,0},{2,3},{3,2},{4,5},{5,4},{6,7},{7,6},{8,9},{9,8},{10,11... | collective-permute-start | bytes 6291464 | tf_op jit(solution)/shard_map/ppermute | solution.py:30
  79.7 3.0 copy-start.1
  79.7 3.6 %copy-start.2 = (bf16[2048]{0:T(1024)(128)(2,1)S(1)}, bf16[2048]{0:T(1024)(128)(2,1)}, u32[]{:S(2)}) copy-start(bf16[2048]{0:T(1024)(128)(2,1)} %param.45) | copy-start | bytes 12292
  79.8 4.2 %copy-start.3 = (bf16[2048]{0:T(1024)(128)(2,1)S(1)}, bf16[2048]{0:T(1024)(128)(2,1)}, u32[]{:S(2)}) copy-start(bf16[2048]{0:T(1024)(128)(2,1)} %param.49) | copy-start | bytes 12292
  81.2 133.5 %collective-permute-start.7 = (bf16[1,256,2048]{2,1,0:T(8,128)(2,1)}, bf16[1,256,2048]{2,1,0:T(8,128)(2,1)}, u32[]{:S(2)}, u32[]{:S(2)}) collective-permute-start(bf16[1,256,2048]{2,1,0:T(8,128)(2,1)} %get-tuple-element.21), channel_id=1, source_target_pairs={{0,2},{1,3},{2,0},{3,1},{4,6},{5,7},{6,4},{7,5},{8,10},{9,11},{10,... | collective-permute-start | bytes 3145736 | tf_op jit(solution)/shard_map/ppermute | solution.py:30
where the time goes:
time: 315 us; the launch traced here: 310 us
  Pallas kernels  246 us (78%)
  waiting for transfers between devices  27.3 us (9%)
  local copies, waits for them, and re-layouts  17.9 us (6%)
  starting transfers between devices  12.1 us (4%)
  other arithmetic  6.45 us (2%)
    pallas_call x1, Pallas kernels, gathered(): pl.pallas_call(functools.partial(gather_weights_kernel, count), in_specs=...  128 us
    pallas_call x1, Pallas kernels, channel_mixer(): pl.pallas_call(functools.partial(ffn_kernel, overlap), in_specs=[vmem] *...  88.7 us
    ppermute x8, waiting for transfers between devices, moved(): return lax.ppermute(block, axis, route)  27.3 us
    pallas_call x1, Pallas kernels, layer(): pl.pallas_call(functools.partial(mix_kernel, sizes), grid_spec=pltpu.Pref...  14.4 us
    ppermute x8, starting transfers between devices, moved(): return lax.ppermute(block, axis, route)  12.1 us
    pallas_call x1, Pallas kernels, layer(): pl.pallas_call(functools.partial(conv_kernel, sizes), grid=(blocks,), in_...  10.8 us
  transfers between devices with their start and end apart: 8, of which 5 were waited for; matrix products, arithmetic and copies ran while one was open for 4% of the time, Pallas kernels for 41%

commit v1 on v0

v1 whole, which is shorter than its diff:
```python
import functools
import types

import jax
import jax.numpy as jnp
from jax import lax
from jax.experimental import pallas as pl
from jax.experimental.pallas import tpu as pltpu
from jax.sharding import PartitionSpec as P

BLOCK = 128
HALO = 16
LANES = 128
SLOTS = 8
TAIL = 16
CHUNK = 256
RING = 4
AHEAD = 2


EPS = 1e-06
OUTER, INNER = "so", "si"
SEQ = (OUTER, INNER)
CHIP, CORE = "tx", "tc"
HEADS = (CHIP, CORE)
MESH = pl.DeviceIdType.MESH
VMEM_BYTES = 64 * 1024 * 1024 - 128 * 1024
FAR = -1e30
F32 = jnp.float32
BF16 = jnp.bfloat16


def silu(x):
    return x / (1.0 + jnp.exp(-x))


def softplus(x):
    return jnp.maximum(x, 0.0) + jnp.log1p(jnp.exp(-jnp.abs(x)))


def exact_dot(a, b):
    return lax.dot_general(
        a, b, (((1,), (0,)), ((), ())), precision=lax.Precision.HIGHEST, preferred_element_type=F32
    )


def exact_across(a, b):
    return lax.dot_general(
        a, b, (((0,), (0,)), ((), ())), precision=lax.Precision.HIGHEST, preferred_element_type=F32
    )


def lower(n):
    rows = lax.broadcasted_iota(jnp.int32, (n, n), 0)
    return rows >= lax.broadcasted_iota(jnp.int32, (n, n), 1)


def spread(columns, heads, dim):
    rows = columns.shape[0]
    parts = []
    if dim >= LANES:
        for h in heads:
            parts.append(jnp.broadcast_to(columns[:, h : h + 1], (rows, dim)))
    else:
        per = LANES // dim
        lane = lax.broadcasted_iota(jnp.int32, (rows, LANES), 1)
        for first in range(0, len(heads), per):
            part = jnp.broadcast_to(columns[:, heads[first] : heads[first] + 1], (rows, LANES))
            for j in range(1, per):
                h = heads[first + j]
                part = jnp.where(lane >= j * dim, columns[:, h : h + 1], part)
            parts.append(part)
    return jnp.concatenate(parts, axis=1)


def unit_rms(values):
    return values * lax.rsqrt(jnp.mean(values * values, axis=-1, keepdims=True) + EPS)


def flipped(value, by):
    return value + by * (1 - 2 * value)


def half_width(columns):
    return (columns // LANES + 1) // 2 * LANES


def greet(partners):
    barrier = pltpu.get_barrier_semaphore()
    for partner in partners:
        pl.semaphore_signal(barrier, inc=1, device_id=partner, device_id_type=MESH)
    pl.semaphore_wait(barrier, len(partners))


def remote(source, target, send, recv, partner):
    copy = pltpu.make_async_remote_copy(
        src_ref=source,
        dst_ref=target,
        send_sem=send,
        recv_sem=recv,
        device_id=partner,
        device_id_type=MESH,
    )
    return copy


def layer_kernel(names, sizes, overlap, *refs):
    r = types.SimpleNamespace(**dict(zip(names, refs, strict=True)))
    (heads_a, dim_a), (heads_b, dim_b), state_len = sizes
    width_a, width_b = heads_a * dim_a, heads_b * dim_b
    width = width_a + width_b
    groups = (
        (list(range(heads_a)), dim_a, width_a, 0, width),
        (list(range(heads_a, heads_a + heads_b)), dim_b, width_b, width_a, width + state_len),
    )
    length, everything = r.values.shape
    blocks = length // BLOCK
    share, features = r.out.shape
    count = lax.axis_size(OUTER)
    z, y = lax.axis_index(OUTER), lax.axis_index(INNER)
    x, c = lax.axis_index(CHIP), lax.axis_index(CORE)
    pair = z % 2
    first_z = z - pair
    position = 2 * z + y
    side = {INNER: 1 - y}
    near = {CORE: 1 - c}
    across = {CHIP: 1 - x}
    one = {OUTER: z + (1 - c) * (1 - 2 * pair), CHIP: flipped(x, c)}
    two = {OUTER: z + c * (1 - 2 * pair), CHIP: flipped(x, 1 - c)}
    line = [{OUTER: (z + d) % count} for d in range(1, count)]
    turn = [{OUTER: (z + d) % count, INNER: 1 - y} for d in (1, count - 1)]
    greet([side, near, across, *line, *turn])

    inputs = (r.small, r.large, r.keys, r.queries)
    column = 0
    halo_columns = []
    for ref in inputs:
        halo_columns.append(pl.ds(column, ref.shape[1]))
        column += ref.shape[1]

    def halo_copy(index, partner):
        return remote(
            inputs[index].at[pl.ds(length - HALO, HALO)],
            r.halo.at[:, halo_columns[index]],
            r.halo_send.at[index],
            r.halo_recv.at[index],
            partner,
        )

    next_z = (z + 1) % count
    last = position == 2 * count - 1

    @pl.when(y == 0)
    def _():
        for index in range(4):
            halo_copy(index, side).start()

    @pl.when((y == 1) & ~last)
    def _():
        for index in range(4):
            halo_copy(index, {OUTER: next_z, INNER: 0}).start()

    loads = []

    def load(source, target):
        copy = pltpu.make_async_copy(source, target, r.load_sem.at[len(loads)])
        copy.start()
        loads.append(copy)

    for index, ref in enumerate(inputs):
        load(ref, r.values.at[:, halo_columns[index]])

    shards = (r.gate_proj, r.up_proj, r.down_proj)
    gathered = (r.gate_all, r.up_all, r.down_all)
    rows, columns = r.gate_proj.shape
    wide = r.gate_all.shape[1]

    def half(m, member):
        start = pl.multiple_of(member * (columns - wide), LANES)
        return shards[m].at[:, pl.ds(start, wide)]

    def piece(m, source):
        return gathered[m].at[pl.ds(pl.multiple_of((source * 2 + y) * rows, rows), rows)]

    def to_line(m, target):
        return remote(half(m, target % 2), piece(m, z), r.send.at[m, target], r.recv.at[m, z], {OUTER: target})

    def from_line(m, source):
        return remote(piece(m, source), piece(m, source), r.send.at[m, source], r.recv.at[m, source], side)

    def own_side(m):
        return remote(half(m, pair), piece(m, z), r.side_send.at[m, z], r.side_recv.at[m, z], side)

    def relay(m, source):
        return remote(
            piece(m, source), piece(m, source), r.side_send.at[m, source], r.side_recv.at[m, source], side
        )

    mate = first_z + 1 - pair
    sources = [mate] + [(first_z + q) % count for q in range(2, count)]

    def pump(m, source):
        from_line(m, source).wait_recv()
        relay(m, source).start()

    for target in sources:
        to_line(0, target).start()
    for m in range(3):
        own_side(m).start()
        load(half(m, pair), piece(m, z))
    load(r.small_gate, r.gates.at[:, pl.ds(0, width_a)])
    load(r.large_gate, r.gates.at[:, pl.ds(width_a, width_b)])
    load(r.small_out, r.out_rows.at[pl.ds(0, width_a)])
    load(r.large_out, r.out_rows.at[pl.ds(width_a, width_b)])
    me = x * 2 + c
    load(r.residual.at[pl.ds(pl.multiple_of(me * share, share), share)], r.out)

    for index in range(4):
        loads[index].wait()

    @pl.when(position > 0)
    def _():
        for index in range(4):
            halo_copy(index, side).wait_recv()
        r.before[...] = r.halo[...]

    @pl.when(position == 0)
    def _():
        r.before[...] = jnp.zeros_like(r.before)

    r.state[...] = jnp.zeros_like(r.state)
    r.total[...] = jnp.zeros_like(r.total)
    causal = lower(BLOCK)
    ones = causal.astype(F32)
    rates = jnp.exp(r.decay[...])

    def block_rows(i):
        return pl.ds(pl.multiple_of(i * BLOCK, BLOCK), BLOCK)

    def convolve(i, _):
        here_rows = block_rows(i)
        taps_len = r.taps.shape[0]
        for start in range(0, everything, LANES):
            here = pl.ds(start, LANES)
            now = r.values[here_rows, here]
            extended = jnp.concatenate([r.before[:, here], now], axis=0).astype(F32)
            summed = None
            for k in range(taps_len):
                first = HALO - taps_len + 1 + k
                term = r.taps[k : k + 1, here] * extended[first : first + BLOCK]
                summed = term if summed is None else summed + term
            r.before[:, here] = now[BLOCK - HALO :]
            r.values[here_rows, here] = silu(summed).astype(BF16)
        dt = softplus(r.steps[here_rows])
        cum = exact_dot(ones, -dt * rates)
        tail = cum[BLOCK - 1 : BLOCK]
        scale = dt * jnp.exp(tail - cum)
        kept = jnp.exp(tail)
        r.logs[here_rows] = r.total[...] + cum
        r.total[...] = r.total[...] + tail
        for heads, dim, size, offset, key_at in groups:
            columns_here = pl.ds(offset, size)
            values = r.values[here_rows, columns_here].astype(F32)
            u = (values * spread(scale, heads, dim)).astype(BF16)
            k = r.values[here_rows, pl.ds(key_at, state_len)]
            fresh = lax.dot_general(k, u, (((0,), (0,)), ((), ())), preferred_element_type=F32)
            old = r.state[:, columns_here]
            r.states[i, :, columns_here] = old.astype(BF16)
            r.state[:, columns_here] = old * spread(kept, heads, dim) + fresh
        return 0

    lax.fori_loop(0, blocks, convolve, 0)

    def pack(target, state, log):
        target[:state_len] = state.astype(BF16)
        high = log.astype(BF16)
        low = (log - high.astype(F32)).astype(BF16)
        row = lax.broadcasted_iota(jnp.int32, (TAIL, width), 0)
        both = jnp.where(row == 0, high.astype(F32), jnp.where(row == 1, low.astype(F32), 0.0))
        target[state_len:] = both.astype(BF16)

    def opened(ref):
        tail = ref[state_len:].astype(F32)
        return ref[:state_len].astype(F32), tail[0:1] + tail[1:2]

    pack(
        r.packed,
        r.state[...],
        jnp.concatenate([spread(r.total[...], heads, dim) for heads, dim, *_ in groups], axis=1),
    )
    pair_copy = remote(r.packed, r.beside, r.state_send.at[0], r.state_recv.at[0], side)
    pair_copy.start()
    for target in sources:
        to_line(1, target).start()

    upper = (
        lax.broadcasted_iota(jnp.int32, (BLOCK, BLOCK), 0)
        <= lax.broadcasted_iota(jnp.int32, (BLOCK, BLOCK), 1)
    ).astype(F32)
    same = (
        lax.broadcasted_iota(jnp.int32, (BLOCK, BLOCK), 0)
        == lax.broadcasted_iota(jnp.int32, (BLOCK, BLOCK), 1)
    ).astype(F32)
    lane = lax.broadcasted_iota(jnp.int32, (BLOCK, LANES), 1)

    def inside_block(i, _):
        here_rows = block_rows(i)
        dt = softplus(r.steps[here_rows])
        log = -dt * rates
        cum = exact_dot(ones, log)
        cum_across = exact_across(log, upper)
        dt_across = exact_across(dt, same)
        grown = jnp.exp(cum)
        for heads, dim, size, offset, key_at in groups:
            columns_here = pl.ds(offset, size)
            values = r.values[here_rows, columns_here]
            k = r.values[here_rows, pl.ds(key_at, state_len)]
            q = r.values[here_rows, pl.ds(key_at + 2 * state_len, state_len)]
            scores = lax.dot_general(q, k, (((1,), (1,)), ((), ())), preferred_element_type=F32)
            carried = jnp.dot(q, r.states[i, :, columns_here], preferred_element_type=F32)
            carried = carried * spread(grown, heads, dim)
            inside = []
            span = max(dim, LANES)
            per = span // dim
            for first in range(0, len(heads), per):
                part_values = values[:, first * dim : first * dim + span]
                part = None
                for j in range(per):
                    h = heads[first + j]
                    gap = cum[:, h : h + 1] - cum_across[h : h + 1]
                    decays = jnp.exp(jnp.where(causal, gap, FAR))
                    w = (scores * decays * dt_across[h : h + 1]).astype(BF16)
                    got = jnp.dot(w, part_values, preferred_element_type=F32)
                    part = got if part is None else jnp.where(lane >= j * dim, got, part)
                inside.append(part)
            r.inner[here_rows, columns_here] = jnp.concatenate(inside, axis=1) + carried
        return 0

    lax.fori_loop(0, blocks // 2, inside_block, 0)

    pair_copy.wait_recv()
    mine, mine_log = opened(r.packed)
    theirs, theirs_log = opened(r.beside)
    front = y == 0
    lead = jnp.where(front, mine, theirs)
    lead_log = jnp.where(front, mine_log, theirs_log)
    trail = jnp.where(front, theirs, mine)
    trail_log = jnp.where(front, theirs_log, mine_log)
    r.both[:state_len] = lead * jnp.exp(trail_log) + trail
    r.both[state_len:] = jnp.broadcast_to(lead_log + trail_log, (8, width))
    r.ahead[:state_len] = lead
    r.ahead[state_len:] = jnp.broadcast_to(lead_log, (8, width))

    def line_copy():
        return remote(r.passed, r.arrived, r.state_send.at[1], r.state_recv.at[1], {OUTER: next_z})

    @pl.when(z == 0)
    def _():
        pack(r.passed, r.both[:state_len], r.both[state_len : state_len + 1])
        line_copy().start()

    lax.fori_loop(blocks // 2, blocks, inside_block, 0)

    @pl.when(z == 0)
    def _():
        r.state[...] = jnp.zeros_like(r.state)

    @pl.when(z > 0)
    def _():
        line_copy().wait_recv()
        before, before_log = opened(r.arrived)
        r.state[...] = before

        @pl.when(z < count - 1)
        def _():
            both_log = r.both[state_len : state_len + 1]
            pack(r.passed, before * jnp.exp(both_log) + r.both[:state_len], before_log + both_log)
            line_copy().start()

    @pl.when(y == 1)
    def _():
        r.state[...] = r.state[...] * jnp.exp(r.ahead[state_len : state_len + 1]) + r.ahead[:state_len]

    r.entering[...] = r.state[...].astype(BF16)
    for target in sources:
        to_line(2, target).start()
    queue = [(m, source) for m in range(2) for source in sources]
    marks = [len(queue) * k // 6 for k in range(7)]

    def pumps(first, end):
        for m, source in queue[marks[first] : marks[end]]:
            pump(m, source)

    pumps(0, 2)
    for index in range(7, len(loads)):
        loads[index].wait()

    def near_mix(index):
        return remote(
            r.mix_core.at[index], r.mix_from.at[index], r.mix_send.at[index], r.mix_recv.at[index], near
        )

    across_mix = remote(r.mix_hop, r.mix_got, r.mix_send.at[2], r.mix_recv.at[2], across)

    per_share = share // BLOCK

    def project(b, _):
        which = b // per_share
        far, other = 1 - which // 2, 1 - which % 2
        source = flipped(x, far) * 2 + flipped(c, other)
        i = source * per_share + b % per_share
        here_rows = block_rows(i)
        grown = jnp.exp(r.logs[here_rows])
        result = None
        for heads, dim, size, offset, key_at in groups:
            columns_here = pl.ds(offset, size)
            q = r.values[here_rows, pl.ds(key_at + 2 * state_len, state_len)]
            carried = jnp.dot(q, r.entering[:, columns_here], preferred_element_type=F32)
            mixed = r.inner[here_rows, columns_here] + carried * spread(grown, heads, dim)
            gated = mixed * silu(r.gates[here_rows, columns_here].astype(F32))
            squares = gated * gated
            span = max(dim, LANES)
            per = span // dim
            normed = []
            for first in range(0, len(heads), per):
                at = first * dim
                part = squares[:, at : at + span]
                means = None
                for j in range(per):
                    if per == 1:
                        means = jnp.sum(part, axis=1, keepdims=True)
                    else:
                        ours = (lane >= j * dim) & (lane < (j + 1) * dim)
                        single = jnp.sum(jnp.where(ours, part, 0.0), axis=1, keepdims=True)
                        means = single if means is None else jnp.where(lane >= j * dim, single, means)
                normed.append(gated[:, at : at + span] * lax.rsqrt(means * (1.0 / dim) + EPS))
            normed = jnp.concatenate(normed, axis=1) * r.gain[:, columns_here]
            product = jnp.dot(normed.astype(BF16), r.out_rows[columns_here], preferred_element_type=F32)
            result = product if result is None else result + product
        part_rows = pl.ds(pl.multiple_of(b % per_share * BLOCK, BLOCK), BLOCK)

        @pl.when(other == 1)
        def _():
            r.mix_core[far, part_rows] = result.astype(BF16)

        @pl.when(other == 0)
        def _():
            r.mix_local[far, part_rows] = result

        @pl.when((other == 1) & (b % per_share == per_share - 1))
        def _():
            near_mix(far).start()

        @pl.when(b == 2 * per_share - 1)
        def _():
            near_mix(1).wait_recv()
            r.mix_hop[...] = (r.mix_local[1] + r.mix_from[1].astype(F32)).astype(BF16)
            across_mix.start()

        return 0

    lax.fori_loop(0, blocks, project, 0)
    pumps(2, 4)
    near_mix(0).wait_recv()
    across_mix.wait_recv()

    def place(core, d_one, d_two):
        dz = d_one * (1 - core) + d_two * core
        dx = d_one * core + d_two * (1 - core)
        return (flipped(pair, dz) * 2 + flipped(x, dx)) * 2 + core

    mine_at = place(c, 0, 0)
    tile = BLOCK // 2

    def norms(i, _):
        here = pl.ds(pl.multiple_of(i * tile, tile), tile)
        mix = r.mix_local[0, here] + r.mix_from[0, here].astype(F32) + r.mix_got[here].astype(F32)
        mixed = r.out[here].astype(F32) + unit_rms(mix) * r.gains[0:1]
        r.mixed[here] = mixed
        r.rows[mine_at, here] = (unit_rms(mixed) * r.gains[1:2]).astype(BF16)
        return 0

    lax.fori_loop(0, share // tile, norms, 0)

    def passing(slot, index, partner):
        return remote(r.rows.at[slot], r.rows.at[slot], r.rows_send.at[index], r.rows_recv.at[slot], partner)

    for index, partner in enumerate((one, two, near)):
        passing(mine_at, index, partner).start()
    pumps(4, 6)
    for m in range(2):
        loads[4 + m].wait()
        for source in range(count):
            relay(m, source).wait_recv()

    def hidden_of(slot):
        values = r.rows[slot]
        gate = jnp.dot(values, r.gate_all[...], preferred_element_type=F32)
        up = jnp.dot(values, r.up_all[...], preferred_element_type=F32)
        hidden = silu(gate) * up
        at = lax.broadcasted_iota(jnp.int32, hidden.shape, 1)
        return jnp.where(at >= pair * overlap, hidden, 0.0).astype(BF16)

    def expand(j, _):
        d_one, d_two = j % 2, j // 2
        slot = place(c, d_one, d_two)

        @pl.when(j > 0)
        def _():
            passing(slot, 0, near).wait_recv()
            passing(slot, 3 + j, near).start()

        @pl.when(j == 1)
        def _():
            passing(slot, 3, two).start()

        r.hidden[j] = hidden_of(slot)
        slot = place(1 - c, d_one, d_two)
        passing(slot, 0, near).wait_recv()
        r.hidden[4 + j] = hidden_of(slot)
        return 0

    lax.fori_loop(0, 4, expand, 0)

    chunk = r.got_one.shape[-1]
    per_chunk = chunk // rows
    chunks = features // chunk
    first_chunk = 2 * first_z * rows // chunk

    def chunk_at(k):
        return (first_chunk + k) % chunks

    def pump_chunk(k):
        for index in range(per_chunk):
            block = chunk_at(k) * per_chunk + index

            @pl.when((block % 2 == y) & (block // 2 != z))
            def _():
                pump(2, block // 2)

    def near_copy(k):
        return remote(
            r.to_core.at[k % RING], r.from_core.at[k], r.core_send.at[k % RING], r.core_recv.at[k], near
        )

    def two_copy(k):
        return remote(r.hop_two.at[k % RING], r.got_two.at[k], r.two_send.at[k % RING], r.two_recv.at[k], two)

    def one_copy(k):
        return remote(r.hop_one.at[k % RING], r.got_one.at[k], r.one_send.at[k % RING], r.one_recv.at[k], one)

    def local_at(k, j):
        slot = k % RING
        start = pl.multiple_of((slot % 2 * 4 + j) * chunk, LANES)
        return slot // 2, slice(None), pl.ds(start, chunk)

    loads[6].wait()
    for k in range(AHEAD):
        pump_chunk(k)

    def reduce_step(k, _):
        @pl.when(k < chunks)
        def _():
            for index in range(per_chunk):
                block = chunk_at(k) * per_chunk + index

                @pl.when(block % 2 != y)
                def _():
                    relay(2, block // 2).wait_recv()

            @pl.when(k >= RING)
            def _():
                near_copy(k).wait_send()

            at = pl.ds(pl.multiple_of(chunk_at(k) * chunk, chunk), chunk)
            weights = r.down_all[at]
            for j in range(4):
                r.to_core[k % RING, j] = lax.dot_general(
                    r.hidden[4 + j], weights, (((1,), (1,)), ((), ())), preferred_element_type=F32
                ).astype(BF16)
            near_copy(k).start()
            for j in range(4):
                r.mix_local[local_at(k, j)] = lax.dot_general(
                    r.hidden[j], weights, (((1,), (1,)), ((), ())), preferred_element_type=F32
                )

        @pl.when((k >= 1) & (k < chunks + 1))
        def _():
            p = k - 1
            near_copy(p).wait_recv()

            @pl.when(p >= RING)
            def _():
                two_copy(p).wait_send()

            for index, j in enumerate((3, 2)):
                total = r.mix_local[local_at(p, j)] + r.from_core[p, j].astype(F32)
                r.hop_two[p % RING, index] = total.astype(BF16)
            two_copy(p).start()
            for j in range(2):
                r.mix_local[local_at(p, j)] = r.mix_local[local_at(p, j)] + r.from_core[p, j].astype(F32)

        @pl.when((k >= 2) & (k < chunks + 2))
        def _():
            p = k - 2
            two_copy(p).wait_recv()

            @pl.when(p >= RING)
            def _():
                one_copy(p).wait_send()

            total = r.mix_local[local_at(p, 1)] + r.got_two[p, 0].astype(F32)
            r.hop_one[p % RING] = total.astype(BF16)
            one_copy(p).start()

        @pl.when(k >= 3)
        def _():
            p = k - 3
            one_copy(p).wait_recv()
            total = r.mix_local[local_at(p, 0)] + r.got_two[p, 1].astype(F32) + r.got_one[p].astype(F32)
            r.ffn[:, pl.ds(pl.multiple_of(chunk_at(p) * chunk, chunk), chunk)] = total

        @pl.when(k < chunks - AHEAD)
        def _():
            pump_chunk(k + AHEAD)

        return 0

    lax.fori_loop(0, chunks + 3, reduce_step, 0)

    def finish(i, _):
        here = pl.ds(pl.multiple_of(i * tile, tile), tile)
        r.out[here] = (r.mixed[here] + 0.5 * unit_rms(r.ffn[here]) * r.gains[2:3]).astype(BF16)
        return 0

    lax.fori_loop(0, share // tile, finish, 0)

    @pl.when(~last)
    def _():
        for index in range(4):
            halo_copy(index, side).wait_send()

    pair_copy.wait_send()

    @pl.when(z < count - 1)
    def _():
        line_copy().wait_send()

    for m in range(3):
        for target in sources:
            to_line(m, target).wait_send()
        for source in range(count):
            relay(m, source).wait_send()
    near_mix(0).wait_send()
    near_mix(1).wait_send()
    across_mix.wait_send()
    for index in range(7):
        passing(mine_at, index, near).wait_send()
    for slot in range(min(RING, chunks)):
        near_copy(slot).wait_send()
        two_copy(slot).wait_send()
        one_copy(slot).wait_send()


def layer(
    residual,
    small_heads,
    large_heads,
    state_keys,
    state_queries,
    small_gate,
    large_gate,
    small_step,
    large_step,
    small_taps,
    large_taps,
    key_taps,
    query_taps,
    small_decay,
    large_decay,
    small_gain,
    large_gain,
    small_out,
    large_out,
    mixer_gain,
    ffn_in_gain,
    gate_proj,
    up_proj,
    down_proj,
    ffn_out_gain,
):
    length, features = residual.shape
    state_len = state_keys.shape[-1]
    key_rows = state_keys.reshape(length, -1)
    query_rows = state_queries.reshape(length, -1)
    heads_a = small_step.shape[1]
    heads_b = large_step.shape[1]
    heads = heads_a + heads_b
    width_a = small_heads.shape[1]
    width_b = large_heads.shape[1]
    width = width_a + width_b
    everything = width + key_rows.shape[1] + query_rows.shape[1]
    sizes = ((heads_a, width_a // heads_a), (heads_b, width_b // heads_b), state_len)
    steps = jnp.pad(
        jnp.concatenate([small_step, large_step], axis=1), ((0, 0), (0, SLOTS - heads))
    )
    decay = jnp.pad(jnp.concatenate([small_decay, large_decay]), (0, SLOTS - heads))
    taps_len = small_taps.shape[0]
    taps = jnp.concatenate(
        [small_taps, large_taps, key_taps.reshape(taps_len, -1), query_taps.reshape(taps_len, -1)],
        axis=1,
    ).astype(F32)
    gain = jnp.concatenate([small_gain, large_gain]).astype(F32)[None]
    gains = jnp.stack([mixer_gain, ffn_in_gain, ffn_out_gain]).astype(F32)
    share = length // lax.axis_size(HEADS)
    rows, columns = down_proj.shape
    count = lax.axis_size(OUTER)
    wide = half_width(columns)
    chunk = max(rows, CHUNK)
    chunks = features // chunk
    blocks = length // BLOCK
    vmem = pl.BlockSpec(memory_space=pltpu.VMEM)
    hbm = pl.BlockSpec(memory_space=pl.ANY)
    dma = pltpu.SemaphoreType.DMA
    operands = {
        "small": (small_heads, hbm),
        "large": (large_heads, hbm),
        "keys": (key_rows, hbm),
        "queries": (query_rows, hbm),
        "small_gate": (small_gate, hbm),
        "large_gate": (large_gate, hbm),
        "small_out": (small_out, hbm),
        "large_out": (large_out, hbm),
        "residual": (residual, hbm),
        "gate_proj": (gate_proj, hbm),
        "up_proj": (up_proj, hbm),
        "down_proj": (down_proj, hbm),
        "steps": (steps, vmem),
        "decay": (decay[None], vmem),
        "taps": (taps, vmem),
        "gain": (gain, vmem),
        "gains": (gains, vmem),
    }
    packed = (state_len + TAIL, width)
    opened = (state_len + 8, width)
    scratch = {
        "values": pltpu.VMEM((length, everything), BF16),
        "gates": pltpu.VMEM((length, width), BF16),
        "out_rows": pltpu.VMEM((width, features), BF16),
        "gate_all": pltpu.VMEM((features, wide), BF16),
        "up_all": pltpu.VMEM((features, wide), BF16),
        "down_all": pltpu.VMEM((features, wide), BF16),
        "halo": pltpu.VMEM((HALO, everything), BF16),
        "before": pltpu.VMEM((HALO, everything), BF16),
        "state": pltpu.VMEM((state_len, width), F32),
        "states": pltpu.VMEM((blocks, state_len, width), BF16),
        "total": pltpu.VMEM((1, SLOTS), F32),
        "logs": pltpu.VMEM((length, SLOTS), F32),
        "inner": pltpu.VMEM((length, width), F32),
        "packed": pltpu.VMEM(packed, BF16),
        "beside": pltpu.VMEM(packed, BF16),
        "passed": pltpu.VMEM(packed, BF16),
        "arrived": pltpu.VMEM(packed, BF16),
        "both": pltpu.VMEM(opened, F32),
        "ahead": pltpu.VMEM(opened, F32),
        "entering": pltpu.VMEM((state_len, width), BF16),
        "mix_core": pltpu.VMEM((2, share, features), BF16),
        "mix_from": pltpu.VMEM((2, share, features), BF16),
        "mix_local": pltpu.VMEM((2, share, features), F32),
        "mix_hop": pltpu.VMEM((share, features), BF16),
        "mix_got": pltpu.VMEM((share, features), BF16),
        "mixed": pltpu.VMEM((share, features), F32),
        "rows": pltpu.VMEM((8, share, features), BF16),
        "hidden": pltpu.VMEM((8, share, wide), BF16),
        "to_core": pltpu.VMEM((RING, 4, share, chunk), BF16),
        "from_core": pltpu.VMEM((chunks, 4, share, chunk), BF16),
        "hop_two": pltpu.VMEM((RING, 2, share, chunk), BF16),
        "got_two": pltpu.VMEM((chunks, 2, share, chunk), BF16),
        "hop_one": pltpu.VMEM((RING, share, chunk), BF16),
        "got_one": pltpu.VMEM((chunks, share, chunk), BF16),
        "ffn": pltpu.VMEM((share, features), F32),
        "halo_send": dma((4,)),
        "halo_recv": dma((4,)),
        "load_sem": dma((12,)),
        "send": dma((3, count)),
        "recv": dma((3, count)),
        "side_send": dma((3, count)),
        "side_recv": dma((3, count)),
        "state_send": dma((2,)),
        "state_recv": dma((2,)),
        "mix_send": dma((3,)),
        "mix_recv": dma((3,)),
        "rows_send": dma((7,)),
        "rows_recv": dma((8,)),
        "core_send": dma((RING,)),
        "core_recv": dma((chunks,)),
        "two_send": dma((RING,)),
        "two_recv": dma((chunks,)),
        "one_send": dma((RING,)),
        "one_recv": dma((chunks,)),
    }
    names = (*operands, "out", *scratch)
    return pl.pallas_call(
        functools.partial(layer_kernel, names, sizes, 2 * wide - columns),
        in_specs=[spec for _, spec in operands.values()],
        out_specs=vmem,
        out_shape=jax.ShapeDtypeStruct((share, features), BF16),
        scratch_shapes=list(scratch.values()),
        compiler_params=pltpu.CompilerParams(
            collective_id=0, has_side_effects=True, vmem_limit_bytes=VMEM_BYTES
        ),
        cost_estimate=pl.CostEstimate(
            flops=40_000_000_000, bytes_accessed=share * features, transcendentals=0
        ),
        name="layer",
    )(*[array for array, _ in operands.values()])


def solution(mesh):
    placed = (
        P(SEQ, None),
        P(SEQ, HEADS),
        P(SEQ, HEADS),
        P(SEQ, HEADS, None),
        P(SEQ, HEADS, None),
        P(SEQ, HEADS),
        P(SEQ, HEADS),
        P(SEQ, HEADS),
        P(SEQ, HEADS),
        P(None, HEADS),
        P(None, HEADS),
        P(None, HEADS, None),
        P(None, HEADS, None),
        P(HEADS),
        P(HEADS),
        P(HEADS),
        P(HEADS),
        P(HEADS, None),
        P(HEADS, None),
        P(),
        P(),
        P(SEQ, HEADS),
        P(SEQ, HEADS),
        P(SEQ, HEADS),
        P(),
    )
    outer, heads = mesh.shape["sp"] // 2, mesh.shape["tp"] // 2
    cut = jax.sharding.Mesh(mesh.devices.reshape(outer, 2, heads, 2), (OUTER, INNER, CHIP, CORE))
    return jax.shard_map(
        layer, mesh=cut, in_specs=placed, out_specs=P((*SEQ, *HEADS), None), check_vma=False
    )
```

time: 315 us -> 249 us (0.79); the launches traced: 310 us -> 248 us
  waiting for transfers between devices: 27.3 us -> 0 us
  starting transfers between devices: 12.1 us -> 0 us
  Pallas kernels: 246 us -> 234 us
  local copies, waits for them, and re-layouts: 17.9 us -> 9.8 us
    ppermute x8 -> x0, waiting for transfers between devices: 27.3 us -> none  [moved(): return lax.ppermute(block, axis, route)]
    pallas_call x5 -> x1, Pallas kernels: 246 us -> 234 us  [layer(): pl.pallas_call(functools.partial(layer_kernel, names, sizes, 2 * wide - c...]
    ppermute x8 -> x0, starting transfers between devices: 12.1 us -> none  [moved(): return lax.ppermute(block, axis, route)]
    slice x5 -> x0, local copies, waits for them, and re-layouts: 4.75 us -> none  [the longest x2 3.36 us: scattered(): other = paired(blocks[half:], axis, bit)]
  transfers between devices with their start and end apart: 8 -> 0, of which waited for: 5 -> 0; matrix products, arithmetic and copies ran while one was open for 4% -> 0% of each run, Pallas kernels for 41% -> 0%
where the time goes in v1:
time: 249 us; the launch traced here: 248 us
  Pallas kernels  234 us (94%)
  local copies, waits for them, and re-layouts  9.8 us (4%)
  other arithmetic  4.51 us (2%)
    pallas_call x1, Pallas kernels, layer(): pl.pallas_call(functools.partial(layer_kernel, names, sizes, 2 * wide - c...  234 us

profile of v1, /device:TPU:24, one launch (start us, length us, event | category | flops | bytes accessed | tf_op | source)
XLA Modules:
  0.0 248.0 jit_solution(16644749311765373687)
XLA Ops:
  0.0 1.3 fusion.1.refs_13_
  1.3 0.7 concatenate.26
  1.9 0.7 concatenate.27
  2.6 0.6 maximum_convert_fusion.2.refs_15_
  3.1 0.7 copy_bitcast_fusion.2
  3.8 0.7 stack.12
  4.5 0.7 stack.13
  5.2 0.7 stack.14
  5.9 0.6 maximum_convert_fusion.refs_16_
  6.6 1.3 maximum_convert_fusion.1.refs_14_
  7.9 0.7 pad_maximum_fusion
  8.6 0.2 copy.28
  8.8 0.8 pad.8.refs_12_
  9.7 2.3 copy_bitcast_fusion
  12.0 233.7 %layer.1 = bf16[256,2048]{1,0:T(8,128)(2,1)} custom-call(bf16[1024,256]{1,0:T(8,128)(2,1)} %refs_0_.1, bf16[1024,256]{1,0:T(8,128)(2,1)} %refs_1_.1, bf16[1024,256]{1,0:T(8,128)(2,1)} %get-tuple-element.8.refs_2_, bf16[1024,256]{1,0:T(8,128)(2,1)} %get-tuple-element.7.refs_3_, bf16[1024,256]{1,0:T(8,128)(2,1)} %refs_4_.1, bf16[1024,256]{1,0:T(8,128)(2,1)} %refs_5_.1, ...), custom_call_target="tpu_custom_call" | custom-call | flops 40000000000 | bytes 524288 | tf_op jit(solution)/shard_map/layer/pallas_call | solution.py:803
  245.7 2.3 copy.38

commit v2 on v1

--- a/solution.py
+++ b/solution.py
@@ -15,7 +15,7 @@
 TAIL = 16
 CHUNK = 256
 RING = 4
-AHEAD = 2
+AHEAD = 3
 
 
 EPS = 1e-06
@@ -125,6 +125,7 @@
     side = {INNER: 1 - y}
     near = {CORE: 1 - c}
     across = {CHIP: 1 - x}
+    upright = {OUTER: first_z + 1 - pair}
     one = {OUTER: z + (1 - c) * (1 - 2 * pair), CHIP: flipped(x, c)}
     two = {OUTER: z + c * (1 - 2 * pair), CHIP: flipped(x, 1 - c)}
     line = [{OUTER: (z + d) % count} for d in range(1, count)]
@@ -170,6 +171,19 @@
     for index, ref in enumerate(inputs):
         load(ref, r.values.at[:, halo_columns[index]])
 
+    for index in range(4):
+        loads[index].wait()
+
+    @pl.when(position > 0)
+    def _():
+        for index in range(4):
+            halo_copy(index, side).wait_recv()
+        r.before[...] = r.halo[...]
+
+    @pl.when(position == 0)
+    def _():
+        r.before[...] = jnp.zeros_like(r.before)
+
     shards = (r.gate_proj, r.up_proj, r.down_proj)
     gathered = (r.gate_all, r.up_all, r.down_all)
     rows, columns = r.gate_proj.shape
@@ -197,16 +211,40 @@
         )
 
     mate = first_z + 1 - pair
-    sources = [mate] + [(first_z + q) % count for q in range(2, count)]
+    lowest = (count - first_z) // count
+    crossing = [lowest * (count + 1 - q) + (1 - lowest) * ((first_z + q) % count) for q in range(2, count)]
+    sources = [*crossing[:1], mate, *crossing[1:]]
+    edge = (z == 0) | (z == count - 1)
 
     def pump(m, source):
         from_line(m, source).wait_recv()
         relay(m, source).start()
 
-    for target in sources:
-        to_line(0, target).start()
+    def start_line(condition, *pieces):
+        @pl.when(condition)
+        def _():
+            for m, target in pieces:
+                to_line(m, target).start()
+
+    outward = [[(m, target) for target in crossing] for m in range(3)]
+    both_outward = [*outward[0], *outward[1]]
+    rest = [*outward[0][1:], (0, mate), (1, mate)]
+    rising = (pair == 0) & ~edge
+    falling = (pair == 1) & ~edge
+    start_line(edge, outward[0][0])
+    start_line(z == count - 1, *rest, *outward[1])
+    start_line(falling, (0, mate), (1, mate))
+    start_line(rising, *both_outward)
+    queue = [(0, crossing[0]), (0, mate), (1, mate)]
+    queue += [(0, source) for source in crossing[1:]] + [(1, source) for source in crossing]
+    marks = [len(queue) * k // 6 for k in range(7)]
+
+    def pumps(first, end):
+        for m, source in queue[marks[first] : marks[end]]:
+            pump(m, source)
+
+    own_side(0).start()
     for m in range(3):
-        own_side(m).start()
         load(half(m, pair), piece(m, z))
     load(r.small_gate, r.gates.at[:, pl.ds(0, width_a)])
     load(r.large_gate, r.gates.at[:, pl.ds(width_a, width_b)])
@@ -215,24 +253,29 @@
     me = x * 2 + c
     load(r.residual.at[pl.ds(pl.multiple_of(me * share, share), share)], r.out)
 
-    for index in range(4):
-        loads[index].wait()
-
-    @pl.when(position > 0)
-    def _():
-        for index in range(4):
-            halo_copy(index, side).wait_recv()
-        r.before[...] = r.halo[...]
-
-    @pl.when(position == 0)
-    def _():
-        r.before[...] = jnp.zeros_like(r.before)
+    r.taps[:, pl.ds(0, width_a)] = r.small_taps[...].astype(F32)
+    r.taps[:, pl.ds(width_a, width_b)] = r.large_taps[...].astype(F32)
+    column = width
+    for ref in (r.key_taps, r.query_taps):
+        for group in range(ref.shape[1]):
+            for k in range(ref.shape[0]):
+                r.taps[k : k + 1, pl.ds(column, state_len)] = ref[k, group : group + 1].astype(F32)
+            column += state_len
+    r.gain[0:1, pl.ds(0, width_a)] = r.small_gain[...].astype(F32)[None]
+    r.gain[0:1, pl.ds(width_a, width_b)] = r.large_gain[...].astype(F32)[None]
+    for index, ref in enumerate((r.mixer_gain, r.ffn_in_gain, r.ffn_out_gain)):
+        r.gains[index : index + 1] = ref[...].astype(F32)[None]
+    lanes = lax.broadcasted_iota(jnp.int32, (1, SLOTS), 1)
+    decay = jnp.zeros((1, SLOTS), F32)
+    for first, heads, ref in ((0, heads_a, r.small_decay), (heads_a, heads_b, r.large_decay)):
+        for h in range(heads):
+            decay = jnp.where(lanes == first + h, ref[h], decay)
 
     r.state[...] = jnp.zeros_like(r.state)
     r.total[...] = jnp.zeros_like(r.total)
     causal = lower(BLOCK)
     ones = causal.astype(F32)
-    rates = jnp.exp(r.decay[...])
+    rates = jnp.exp(decay)
 
     def block_rows(i):
         return pl.ds(pl.multiple_of(i * BLOCK, BLOCK), BLOCK)
@@ -290,8 +333,7 @@
     )
     pair_copy = remote(r.packed, r.beside, r.state_send.at[0], r.state_recv.at[0], side)
     pair_copy.start()
-    for target in sources:
-        to_line(1, target).start()
+    own_side(1).start()
 
     upper = (
         lax.broadcasted_iota(jnp.int32, (BLOCK, BLOCK), 0)
@@ -350,48 +392,42 @@
     r.both[state_len:] = jnp.broadcast_to(lead_log + trail_log, (8, width))
     r.ahead[:state_len] = lead
     r.ahead[state_len:] = jnp.broadcast_to(lead_log, (8, width))
-
-    def line_copy():
-        return remote(r.passed, r.arrived, r.state_send.at[1], r.state_recv.at[1], {OUTER: next_z})
-
-    @pl.when(z == 0)
-    def _():
-        pack(r.passed, r.both[:state_len], r.both[state_len : state_len + 1])
-        line_copy().start()
-
-    lax.fori_loop(blocks // 2, blocks, inside_block, 0)
-
-    @pl.when(z == 0)
-    def _():
-        r.state[...] = jnp.zeros_like(r.state)
-
-    @pl.when(z > 0)
-    def _():
-        line_copy().wait_recv()
-        before, before_log = opened(r.arrived)
-        r.state[...] = before
-
-        @pl.when(z < count - 1)
-        def _():
-            both_log = r.both[state_len : state_len + 1]
-            pack(r.passed, before * jnp.exp(both_log) + r.both[:state_len], before_log + both_log)
-            line_copy().start()
+    r.state[...] = jnp.zeros_like(r.state)
+    r.before_log[...] = jnp.zeros_like(r.before_log)
+    hops = r.passed.shape[0]
+
+    def line_copy(s):
+        target = {OUTER: (z + (1 << s)) % count}
+        return remote(r.passed.at[s], r.arrived.at[s], r.line_send.at[s], r.line_recv.at[s], target)
+
+    for s in range(hops):
+
+        @pl.when(z + (1 << s) < count)
+        def _():
+            pack(r.passed.at[s], r.both[:state_len], r.both[state_len : state_len + 1])
+            line_copy(s).start()
+
+        if s == 0:
+            lax.fori_loop(blocks // 2, blocks, inside_block, 0)
+        if s == hops - 1:
+            start_line(z == 0, *rest)
+            start_line(falling, *both_outward)
+
+        @pl.when(z >= 1 << s)
+        def _():
+            line_copy(s).wait_recv()
+            before, before_log = opened(r.arrived.at[s])
+            r.state[...] = before * jnp.exp(r.before_log[0:1]) + r.state[...]
+            r.before_log[...] = r.before_log[...] + before_log
+            r.both[:state_len] = before * jnp.exp(r.both[state_len : state_len + 1]) + r.both[:state_len]
+            r.both[state_len:] = r.both[state_len:] + before_log
 
     @pl.when(y == 1)
     def _():
         r.state[...] = r.state[...] * jnp.exp(r.ahead[state_len : state_len + 1]) + r.ahead[:state_len]
 
     r.entering[...] = r.state[...].astype(BF16)
-    for target in sources:
-        to_line(2, target).start()
-    queue = [(m, source) for m in range(2) for source in sources]
-    marks = [len(queue) * k // 6 for k in range(7)]
-
-    def pumps(first, end):
-        for m, source in queue[marks[first] : marks[end]]:
-            pump(m, source)
-
-    pumps(0, 2)
+    start_line(rising, (0, mate), (1, mate))
     for index in range(7, len(loads)):
         loads[index].wait()
 
@@ -460,14 +496,12 @@
         return 0
 
     lax.fori_loop(0, blocks, project, 0)
-    pumps(2, 4)
+    pumps(0, 4)
     near_mix(0).wait_recv()
     across_mix.wait_recv()
 
     def place(core, d_one, d_two):
-        dz = d_one * (1 - core) + d_two * core
-        dx = d_one * core + d_two * (1 - core)
-        return (flipped(pair, dz) * 2 + flipped(x, dx)) * 2 + core
+        return (flipped(pair, d_one) * 2 + flipped(x, d_two)) * 2 + core
 
     mine_at = place(c, 0, 0)
     tile = BLOCK // 2
@@ -485,23 +519,27 @@
     def passing(slot, index, partner):
         return remote(r.rows.at[slot], r.rows.at[slot], r.rows_send.at[index], r.rows_recv.at[slot], partner)
 
-    for index, partner in enumerate((one, two, near)):
+    for index, partner in enumerate((upright, across, near)):
         passing(mine_at, index, partner).start()
+    start_line(z == 0, *outward[1])
     pumps(4, 6)
-    for m in range(2):
+    own_side(2).start()
+
+    def complete(m):
         loads[4 + m].wait()
         for source in range(count):
             relay(m, source).wait_recv()
 
-    def hidden_of(slot):
-        values = r.rows[slot]
-        gate = jnp.dot(values, r.gate_all[...], preferred_element_type=F32)
-        up = jnp.dot(values, r.up_all[...], preferred_element_type=F32)
-        hidden = silu(gate) * up
-        at = lax.broadcasted_iota(jnp.int32, hidden.shape, 1)
-        return jnp.where(at >= pair * overlap, hidden, 0.0).astype(BF16)
-
-    def expand(j, _):
+    def kept_at(core, j):
+        return (1 - core) * j + core * (j % 2 * 2 + j // 2)
+
+    complete(0)
+
+    def open_gate(slot, at):
+        gate = jnp.dot(r.rows[slot], r.gate_all[...], preferred_element_type=F32)
+        r.hidden[at] = silu(gate).astype(BF16)
+
+    def gates(j, _):
         d_one, d_two = j % 2, j // 2
         slot = place(c, d_one, d_two)
 
@@ -512,15 +550,37 @@
 
         @pl.when(j == 1)
         def _():
-            passing(slot, 3, two).start()
-
-        r.hidden[j] = hidden_of(slot)
+            passing(slot, 3, across).start()
+            to_line(2, mate).start()
+
+            @pl.when(first_z > 0)
+            def _():
+                for m, target in outward[2]:
+                    to_line(m, target).start()
+
+        open_gate(slot, kept_at(c, j))
         slot = place(1 - c, d_one, d_two)
         passing(slot, 0, near).wait_recv()
-        r.hidden[4 + j] = hidden_of(slot)
+        open_gate(slot, 4 + kept_at(1 - c, j))
         return 0
 
-    lax.fori_loop(0, 4, expand, 0)
+    lax.fori_loop(0, 3, gates, 0)
+    complete(1)
+
+    def expand(j, _):
+        for core, first in ((c, 0), (1 - c, 4)):
+            at = first + kept_at(core, j)
+            up = jnp.dot(r.rows[place(core, j % 2, j // 2)], r.up_all[...], preferred_element_type=F32)
+            hidden = r.hidden[at].astype(F32) * up
+            column = lax.broadcasted_iota(jnp.int32, hidden.shape, 1)
+            r.hidden[at] = jnp.where(column >= pair * overlap, hidden, 0.0).astype(BF16)
+        return 0
+
+    lax.fori_loop(0, 3, expand, 0)
+    start_line(first_z == 0, *outward[2])
+    pump(2, mate)
+    lax.fori_loop(3, 4, gates, 0)
+    lax.fori_loop(3, 4, expand, 0)
 
     chunk = r.got_one.shape[-1]
     per_chunk = chunk // rows
@@ -534,7 +594,7 @@
         for index in range(per_chunk):
             block = chunk_at(k) * per_chunk + index
 
-            @pl.when((block % 2 == y) & (block // 2 != z))
+            @pl.when((block % 2 == y) & (block // 2 // 2 != z // 2))
             def _():
                 pump(2, block // 2)
 
@@ -642,9 +702,11 @@
 
     pair_copy.wait_send()
 
-    @pl.when(z < count - 1)
-    def _():
-        line_copy().wait_send()
+    for s in range(hops):
+
+        @pl.when(z + (1 << s) < count)
+        def _():
+            line_copy(s).wait_send()
 
     for m in range(3):
         for target in sources:
@@ -704,14 +766,7 @@
     steps = jnp.pad(
         jnp.concatenate([small_step, large_step], axis=1), ((0, 0), (0, SLOTS - heads))
     )
-    decay = jnp.pad(jnp.concatenate([small_decay, large_decay]), (0, SLOTS - heads))
     taps_len = small_taps.shape[0]
-    taps = jnp.concatenate(
-        [small_taps, large_taps, key_taps.reshape(taps_len, -1), query_taps.reshape(taps_len, -1)],
-        axis=1,
-    ).astype(F32)
-    gain = jnp.concatenate([small_gain, large_gain]).astype(F32)[None]
-    gains = jnp.stack([mixer_gain, ffn_in_gain, ffn_out_gain]).astype(F32)
     share = length // lax.axis_size(HEADS)
     rows, columns = down_proj.shape
     count = lax.axis_size(OUTER)
@@ -721,6 +776,7 @@
     blocks = length // BLOCK
     vmem = pl.BlockSpec(memory_space=pltpu.VMEM)
     hbm = pl.BlockSpec(memory_space=pl.ANY)
+    smem = pl.BlockSpec(memory_space=pltpu.SMEM)
     dma = pltpu.SemaphoreType.DMA
     operands = {
         "small": (small_heads, hbm),
@@ -736,13 +792,21 @@
         "up_proj": (up_proj, hbm),
         "down_proj": (down_proj, hbm),
         "steps": (steps, vmem),
-        "decay": (decay[None], vmem),
-        "taps": (taps, vmem),
-        "gain": (gain, vmem),
-        "gains": (gains, vmem),
+        "small_decay": (small_decay, smem),
+        "large_decay": (large_decay, smem),
+        "small_taps": (small_taps, vmem),
+        "large_taps": (large_taps, vmem),
+        "key_taps": (key_taps, vmem),
+        "query_taps": (query_taps, vmem),
+        "small_gain": (small_gain, vmem),
+        "large_gain": (large_gain, vmem),
+        "mixer_gain": (mixer_gain, vmem),
+        "ffn_in_gain": (ffn_in_gain, vmem),
+        "ffn_out_gain": (ffn_out_gain, vmem),
     }
     packed = (state_len + TAIL, width)
     opened = (state_len + 8, width)
+    hops = max(1, (count - 1).bit_length())
     scratch = {
         "values": pltpu.VMEM((length, everything), BF16),
         "gates": pltpu.VMEM((length, width), BF16),
@@ -750,6 +814,9 @@
         "gate_all": pltpu.VMEM((features, wide), BF16),
         "up_all": pltpu.VMEM((features, wide), BF16),
         "down_all": pltpu.VMEM((features, wide), BF16),
+        "taps": pltpu.VMEM((taps_len, everything), F32),
+        "gain": pltpu.VMEM((1, width), F32),
+        "gains": pltpu.VMEM((3, features), F32),
         "halo": pltpu.VMEM((HALO, everything), BF16),
         "before": pltpu.VMEM((HALO, everything), BF16),
         "state": pltpu.VMEM((state_len, width), F32),
@@ -759,8 +826,9 @@
         "inner": pltpu.VMEM((length, width), F32),
         "packed": pltpu.VMEM(packed, BF16),
         "beside": pltpu.VMEM(packed, BF16),
-        "passed": pltpu.VMEM(packed, BF16),
-        "arrived": pltpu.VMEM(packed, BF16),
+        "passed": pltpu.VMEM((hops, *packed), BF16),
+        "arrived": pltpu.VMEM((hops, *packed), BF16),
+        "before_log": pltpu.VMEM((8, width), F32),
         "both": pltpu.VMEM(opened, F32),
         "ahead": pltpu.VMEM(opened, F32),
         "entering": pltpu.VMEM((state_len, width), BF16),
@@ -786,8 +854,10 @@
         "recv": dma((3, count)),
         "side_send": dma((3, count)),
         "side_recv": dma((3, count)),
-        "state_send": dma((2,)),
-        "state_recv": dma((2,)),
+        "state_send": dma((1,)),
+        "state_recv": dma((1,)),
+        "line_send": dma((hops,)),
+        "line_recv": dma((hops,)),
         "mix_send": dma((3,)),
         "mix_recv": dma((3,)),
         "rows_send": dma((7,)),
@@ -846,6 +916,4 @@
     )
     outer, heads = mesh.shape["sp"] // 2, mesh.shape["tp"] // 2
     cut = jax.sharding.Mesh(mesh.devices.reshape(outer, 2, heads, 2), (OUTER, INNER, CHIP, CORE))
-    return jax.shard_map(
-        layer, mesh=cut, in_specs=placed, out_specs=P((*SEQ, *HEADS), None), check_vma=False
-    )
+    return jax.shard_map(layer, mesh=cut, in_specs=placed, out_specs=P((*SEQ, *HEADS), None), check_vma=False)

time: 249 us -> 199 us (0.80)
  Pallas kernels: 234 us -> 190 us
  local copies, waits for them, and re-layouts: 9.8 us -> 5.72 us
  other arithmetic: 4.51 us -> 0.74 us
    pallas_call x1, Pallas kernels: 234 us -> 190 us  [layer(): pl.pallas_call(functools.partial(layer_kernel, names, sizes, 2 * wide - c...]
    convert_element_type x3 -> x0, other arithmetic: 2.52 us -> none  [the longest x1 1.3 us: layer(): taps = jnp.concatenate([small_taps, large_taps, key_taps.reshape(taps_len...]
where the time goes in v2:
time: 199 us; the launch traced here: 197 us
  Pallas kernels  190 us (95%)
  local copies, waits for them, and re-layouts  5.72 us (3%)
    pallas_call x1, Pallas kernels, layer(): pl.pallas_call(functools.partial(layer_kernel, names, sizes, 2 * wide - c...  190 us

profile of v2, /device:TPU:24, one launch (start us, length us, event | category | flops | bytes accessed | tf_op | source)
XLA Modules:
  0.0 196.6 jit_solution(10356531630829218658)
XLA Ops:
  0.0 0.7 pad_maximum_fusion
  0.7 0.2 copy.28
  1.0 0.9 pad.4.refs_12_
  1.8 2.3 %copy_bitcast_fusion = (bf16[1024,256]{1,0:T(8,128)(2,1)}, bf16[1024,256]{1,0:T(8,128)(2,1)}) fusion(bf16[128,8,2,128]{3,2,1,0:T(2,128)(2,1)} %bitcast.6, bf16[128,8,2,128]{3,2,1,0:T(2,128)(2,1)} %bitcast.7), kind=kLoop, calls=%fused_computation | loop fusion | bytes 2097152 | tf_op jit(solution)/shard_map/reshape | solution.py:757
  4.2 190.1 %layer.1 = bf16[256,2048]{1,0:T(8,128)(2,1)} custom-call(bf16[1024,256]{1,0:T(8,128)(2,1)} %refs_0_.1, bf16[1024,256]{1,0:T(8,128)(2,1)} %refs_1_.1, bf16[1024,256]{1,0:T(8,128)(2,1)} %get-tuple-element.6.refs_2_, bf16[1024,256]{1,0:T(8,128)(2,1)} %get-tuple-element.5.refs_3_, bf16[1024,256]{1,0:T(8,128)(2,1)} %refs_4_.1, bf16[1024,256]{1,0:T(8,128)(2,1)} %refs_5_.1, ...), custom_call_target="tpu_custom_call" | custom-call | flops 40000000000 | bytes 524288 | tf_op jit(solution)/shard_map/layer/pallas_call | solution.py:873
  194.3 2.3 %copy.34 = bf16[256,2048]{1,0:T(8,128)(2,1)} copy(bf16[256,2048]{1,0:T(8,128)(2,1)} %layer.1) | data formatting | bytes 2097152

commit v3 on v2

--- a/solution.py
+++ b/solution.py
@@ -15,7 +15,7 @@
 TAIL = 16
 CHUNK = 256
 RING = 4
-AHEAD = 3
+AHEAD = 4
 
 
 EPS = 1e-06
@@ -104,7 +104,7 @@
     return copy
 
 
-def layer_kernel(names, sizes, overlap, *refs):
+def layer_kernel(names, sizes, base, *refs):
     r = types.SimpleNamespace(**dict(zip(names, refs, strict=True)))
     (heads_a, dim_a), (heads_b, dim_b), state_len = sizes
     width_a, width_b = heads_a * dim_a, heads_b * dim_b
@@ -189,37 +189,98 @@
     rows, columns = r.gate_proj.shape
     wide = r.gate_all.shape[1]
 
-    def half(m, member):
-        start = pl.multiple_of(member * (columns - wide), LANES)
-        return shards[m].at[:, pl.ds(start, wide)]
-
-    def piece(m, source):
-        return gathered[m].at[pl.ds(pl.multiple_of((source * 2 + y) * rows, rows), rows)]
+    extra = wide - base
+
+    def half(m, member, part):
+        if part:
+            return shards[m].at[:, pl.ds(base, extra)]
+        return shards[m].at[:, pl.ds(pl.multiple_of(member * (columns - base), LANES), base)]
+
+    def piece(m, source, part):
+        here = pl.ds(pl.multiple_of((source * 2 + y) * rows, rows), rows)
+        return gathered[m].at[here, pl.ds(base, extra) if part else pl.ds(0, base)]
+
+    class Pieces:
+        def __init__(self, make, member):
+            self.make, self.member = make, member
+
+        def each(self, act):
+            act(self.make(0))
+            if extra:
+
+                @pl.when((self.member + c) % 2 == 0)
+                def _():
+                    act(self.make(1))
+
+        def start(self):
+            self.each(lambda copy: copy.start())
+
+        def wait_send(self):
+            self.each(lambda copy: copy.wait_send())
+
+        def wait_recv(self):
+            self.each(lambda copy: copy.wait_recv())
+
+        def wait(self):
+            self.each(lambda copy: copy.wait())
 
     def to_line(m, target):
-        return remote(half(m, target % 2), piece(m, z), r.send.at[m, target], r.recv.at[m, z], {OUTER: target})
+        def make(p):
+            return remote(
+                half(m, target % 2, p),
+                piece(m, z, p),
+                r.send.at[p, m, target],
+                r.recv.at[p, m, z],
+                {OUTER: target},
+            )
+
+        return Pieces(make, target)
+
+    def sideways(m, source, own, receiving):
+        def make(p):
+            there = piece(m, source, p)
+            here = half(m, pair, p) if own else there
+            sems = (r.send, r.recv) if receiving else (r.side_send, r.side_recv)
+            return remote(here, there, sems[0].at[p, m, source], sems[1].at[p, m, source], side)
+
+        return Pieces(make, z)
 
     def from_line(m, source):
-        return remote(piece(m, source), piece(m, source), r.send.at[m, source], r.recv.at[m, source], side)
+        return sideways(m, source, False, True)
 
     def own_side(m):
-        return remote(half(m, pair), piece(m, z), r.side_send.at[m, z], r.side_recv.at[m, z], side)
+        return sideways(m, z, True, False)
 
     def relay(m, source):
-        return remote(
-            piece(m, source), piece(m, source), r.side_send.at[m, source], r.side_recv.at[m, source], side
+        return sideways(m, source, False, False)
+
+    def own_load(m):
+        return Pieces(
+            lambda p: pltpu.make_async_copy(half(m, pair, p), piece(m, z, p), r.own_sem.at[p, m]), z
         )
+
+    if extra:
+
+        @pl.when((z + c) % 2 == 1)
+        def _():
+            for ref in gathered:
+                ref[:, pl.ds(base, extra)] = jnp.zeros((features, extra), BF16)
 
     mate = first_z + 1 - pair
     lowest = (count - first_z) // count
     crossing = [lowest * (count + 1 - q) + (1 - lowest) * ((first_z + q) % count) for q in range(2, count)]
     sources = [*crossing[:1], mate, *crossing[1:]]
-    edge = (z == 0) | (z == count - 1)
 
     def pump(m, source):
         from_line(m, source).wait_recv()
         relay(m, source).start()
 
+    edge = (z == 0) | (z == count - 1)
+
+    def pump(m, source):
+        from_line(m, source).wait_recv()
+        relay(m, source).start()
+
     def start_line(condition, *pieces):
         @pl.when(condition)
         def _():
@@ -229,9 +290,11 @@
     outward = [[(m, target) for target in crossing] for m in range(3)]
     both_outward = [*outward[0], *outward[1]]
     rest = [*outward[0][1:], (0, mate), (1, mate)]
+    early = [(1, mate), *outward[0][1:], outward[1][0]]
     rising = (pair == 0) & ~edge
     falling = (pair == 1) & ~edge
     start_line(edge, outward[0][0])
+    start_line(z == 0, (0, mate))
     start_line(z == count - 1, *rest, *outward[1])
     start_line(falling, (0, mate), (1, mate))
     start_line(rising, *both_outward)
@@ -245,7 +308,7 @@
 
     own_side(0).start()
     for m in range(3):
-        load(half(m, pair), piece(m, z))
+        own_load(m).start()
     load(r.small_gate, r.gates.at[:, pl.ds(0, width_a)])
     load(r.large_gate, r.gates.at[:, pl.ds(width_a, width_b)])
     load(r.small_out, r.out_rows.at[pl.ds(0, width_a)])
@@ -334,6 +397,7 @@
     pair_copy = remote(r.packed, r.beside, r.state_send.at[0], r.state_recv.at[0], side)
     pair_copy.start()
     own_side(1).start()
+    own_side(2).start()
 
     upper = (
         lax.broadcasted_iota(jnp.int32, (BLOCK, BLOCK), 0)
@@ -410,7 +474,7 @@
         if s == 0:
             lax.fori_loop(blocks // 2, blocks, inside_block, 0)
         if s == hops - 1:
-            start_line(z == 0, *rest)
+            start_line(z == 0, *early)
             start_line(falling, *both_outward)
 
         @pl.when(z >= 1 << s)
@@ -428,7 +492,7 @@
 
     r.entering[...] = r.state[...].astype(BF16)
     start_line(rising, (0, mate), (1, mate))
-    for index in range(7, len(loads)):
+    for index in range(4, len(loads)):
         loads[index].wait()
 
     def near_mix(index):
@@ -521,12 +585,14 @@
 
     for index, partner in enumerate((upright, across, near)):
         passing(mine_at, index, partner).start()
-    start_line(z == 0, *outward[1])
+    start_line(z == 0, *outward[1][1:])
+    to_line(2, mate).start()
+    for m, target in outward[2][1:]:
+        to_line(m, target).start()
     pumps(4, 6)
-    own_side(2).start()
 
     def complete(m):
-        loads[4 + m].wait()
+        own_load(m).wait()
         for source in range(count):
             relay(m, source).wait_recv()
 
@@ -551,12 +617,7 @@
         @pl.when(j == 1)
         def _():
             passing(slot, 3, across).start()
-            to_line(2, mate).start()
-
-            @pl.when(first_z > 0)
-            def _():
-                for m, target in outward[2]:
-                    to_line(m, target).start()
+            start_line(first_z > 0, outward[2][0])
 
         open_gate(slot, kept_at(c, j))
         slot = place(1 - c, d_one, d_two)
@@ -573,11 +634,12 @@
             up = jnp.dot(r.rows[place(core, j % 2, j // 2)], r.up_all[...], preferred_element_type=F32)
             hidden = r.hidden[at].astype(F32) * up
             column = lax.broadcasted_iota(jnp.int32, hidden.shape, 1)
-            r.hidden[at] = jnp.where(column >= pair * overlap, hidden, 0.0).astype(BF16)
+            held = wide - (z + c) % 2 * extra
+            r.hidden[at] = jnp.where(column < held, hidden, 0.0).astype(BF16)
         return 0
 
     lax.fori_loop(0, 3, expand, 0)
-    start_line(first_z == 0, *outward[2])
+    start_line(first_z == 0, outward[2][0])
     pump(2, mate)
     lax.fori_loop(3, 4, gates, 0)
     lax.fori_loop(3, 4, expand, 0)
@@ -614,7 +676,7 @@
         start = pl.multiple_of((slot % 2 * 4 + j) * chunk, LANES)
         return slot // 2, slice(None), pl.ds(start, chunk)
 
-    loads[6].wait()
+    own_load(2).wait()
     for k in range(AHEAD):
         pump_chunk(k)
 
@@ -849,11 +911,12 @@
         "ffn": pltpu.VMEM((share, features), F32),
         "halo_send": dma((4,)),
         "halo_recv": dma((4,)),
-        "load_sem": dma((12,)),
-        "send": dma((3, count)),
-        "recv": dma((3, count)),
-        "side_send": dma((3, count)),
-        "side_recv": dma((3, count)),
+        "load_sem": dma((9,)),
+        "own_sem": dma((2, 3)),
+        "send": dma((2, 3, count)),
+        "recv": dma((2, 3, count)),
+        "side_send": dma((2, 3, count)),
+        "side_recv": dma((2, 3, count)),
         "state_send": dma((1,)),
         "state_recv": dma((1,)),
         "line_send": dma((hops,)),
@@ -871,7 +934,7 @@
     }
     names = (*operands, "out", *scratch)
     return pl.pallas_call(
-        functools.partial(layer_kernel, names, sizes, 2 * wide - columns),
+        functools.partial(layer_kernel, names, sizes, columns - wide),
         in_specs=[spec for _, spec in operands.values()],
         out_specs=vmem,
         out_shape=jax.ShapeDtypeStruct((share, features), BF16),
@@ -916,4 +979,6 @@
     )
     outer, heads = mesh.shape["sp"] // 2, mesh.shape["tp"] // 2
     cut = jax.sharding.Mesh(mesh.devices.reshape(outer, 2, heads, 2), (OUTER, INNER, CHIP, CORE))
-    return jax.shard_map(layer, mesh=cut, in_specs=placed, out_specs=P((*SEQ, *HEADS), None), check_vma=False)
+    return jax.shard_map(
+        layer, mesh=cut, in_specs=placed, out_specs=P((*SEQ, *HEADS), None), check_vma=False
+    )

time: 199 us -> 178 us (0.89)
  Pallas kernels: 190 us -> 170 us
    pallas_call x1, Pallas kernels: 190 us -> 170 us  [layer(): pl.pallas_call(functools.partial(layer_kernel, names, sizes, columns - wi...]
where the time goes in v3:
time: 178 us; the launch traced here: 176 us
  Pallas kernels  170 us (96%)
  local copies, waits for them, and re-layouts  5.72 us (3%)
    pallas_call x1, Pallas kernels, layer(): pl.pallas_call(functools.partial(layer_kernel, names, sizes, columns - wi...  170 us

profile of v3, /device:TPU:24, one launch (start us, length us, event | category | flops | bytes accessed | tf_op | source)
XLA Modules:
  0.0 176.3 jit_solution(12198622939760520828)
XLA Ops:
  0.0 0.7 pad_maximum_fusion
  0.7 0.2 copy.28
  1.0 0.9 pad.4.refs_12_
  1.8 2.3 %copy_bitcast_fusion = (bf16[1024,256]{1,0:T(8,128)(2,1)}, bf16[1024,256]{1,0:T(8,128)(2,1)}) fusion(bf16[128,8,2,128]{3,2,1,0:T(2,128)(2,1)} %bitcast.6, bf16[128,8,2,128]{3,2,1,0:T(2,128)(2,1)} %bitcast.7), kind=kLoop, calls=%fused_computation | loop fusion | bytes 2097152 | tf_op jit(solution)/shard_map/reshape | solution.py:819
  4.2 169.8 %layer.1 = bf16[256,2048]{1,0:T(8,128)(2,1)} custom-call(bf16[1024,256]{1,0:T(8,128)(2,1)} %refs_0_.1, bf16[1024,256]{1,0:T(8,128)(2,1)} %refs_1_.1, bf16[1024,256]{1,0:T(8,128)(2,1)} %get-tuple-element.6.refs_2_, bf16[1024,256]{1,0:T(8,128)(2,1)} %get-tuple-element.5.refs_3_, bf16[1024,256]{1,0:T(8,128)(2,1)} %refs_4_.1, bf16[1024,256]{1,0:T(8,128)(2,1)} %refs_5_.1, ...), custom_call_target="tpu_custom_call" | custom-call | flops 40000000000 | bytes 524288 | tf_op jit(solution)/shard_map/layer/pallas_call | solution.py:936
  174.0 2.3 %copy.34 = bf16[256,2048]{1,0:T(8,128)(2,1)} copy(bf16[256,2048]{1,0:T(8,128)(2,1)} %layer.1) | data formatting | bytes 2097152

commit v4 on v3

--- a/solution.py
+++ b/solution.py
@@ -31,7 +31,8 @@
 
 
 def silu(x):
-    return x / (1.0 + jnp.exp(-x))
+    half = 0.5 * x
+    return half + half * jnp.tanh(half)
 
 
 def softplus(x):
@@ -495,20 +496,34 @@
     for index in range(4, len(loads)):
         loads[index].wait()
 
-    def near_mix(index):
+    per_share = share // BLOCK
+
+    def strip(part):
+        return pl.ds(pl.multiple_of(part * BLOCK, BLOCK), BLOCK)
+
+    def near_mix(index, part):
         return remote(
-            r.mix_core.at[index], r.mix_from.at[index], r.mix_send.at[index], r.mix_recv.at[index], near
+            r.mix_core.at[index, strip(part)],
+            r.mix_from.at[index, strip(part)],
+            r.mix_send.at[index, part],
+            r.mix_recv.at[index, part],
+            near,
         )
 
-    across_mix = remote(r.mix_hop, r.mix_got, r.mix_send.at[2], r.mix_recv.at[2], across)
-
-    per_share = share // BLOCK
+    def across_mix(part):
+        return remote(
+            r.mix_hop.at[strip(part)],
+            r.mix_got.at[strip(part)],
+            r.mix_send.at[2, part],
+            r.mix_recv.at[2, part],
+            across,
+        )
 
     def project(b, _):
-        which = b // per_share
-        far, other = 1 - which // 2, 1 - which % 2
+        far, other = 1 - b // (2 * per_share), 1 - b % 2
+        piece_at = b % (2 * per_share) // 2
         source = flipped(x, far) * 2 + flipped(c, other)
-        i = source * per_share + b % per_share
+        i = source * per_share + piece_at
         here_rows = block_rows(i)
         grown = jnp.exp(r.logs[here_rows])
         result = None
@@ -537,7 +552,8 @@
             normed = jnp.concatenate(normed, axis=1) * r.gain[:, columns_here]
             product = jnp.dot(normed.astype(BF16), r.out_rows[columns_here], preferred_element_type=F32)
             result = product if result is None else result + product
-        part_rows = pl.ds(pl.multiple_of(b % per_share * BLOCK, BLOCK), BLOCK)
+        part = piece_at
+        part_rows = strip(part)
 
         @pl.when(other == 1)
         def _():
@@ -547,22 +563,21 @@
         def _():
             r.mix_local[far, part_rows] = result
 
-        @pl.when((other == 1) & (b % per_share == per_share - 1))
-        def _():
-            near_mix(far).start()
-
-        @pl.when(b == 2 * per_share - 1)
-        def _():
-            near_mix(1).wait_recv()
-            r.mix_hop[...] = (r.mix_local[1] + r.mix_from[1].astype(F32)).astype(BF16)
-            across_mix.start()
+        @pl.when(other == 1)
+        def _():
+            near_mix(far, part).start()
+
+        @pl.when((far == 1) & (other == 0))
+        def _():
+            near_mix(1, part).wait_recv()
+            total = r.mix_local[1, part_rows] + r.mix_from[1, part_rows].astype(F32)
+            r.mix_hop[part_rows] = total.astype(BF16)
+            across_mix(part).start()
 
         return 0
 
     lax.fori_loop(0, blocks, project, 0)
-    pumps(0, 4)
-    near_mix(0).wait_recv()
-    across_mix.wait_recv()
+    pumps(0, 2)
 
     def place(core, d_one, d_two):
         return (flipped(pair, d_one) * 2 + flipped(x, d_two)) * 2 + core
@@ -578,18 +593,30 @@
         r.rows[mine_at, here] = (unit_rms(mixed) * r.gains[1:2]).astype(BF16)
         return 0
 
-    lax.fori_loop(0, share // tile, norms, 0)
-
-    def passing(slot, index, partner):
-        return remote(r.rows.at[slot], r.rows.at[slot], r.rows_send.at[index], r.rows_recv.at[slot], partner)
-
-    for index, partner in enumerate((upright, across, near)):
-        passing(mine_at, index, partner).start()
+    def passing(slot, index, partner, part):
+        here = r.rows.at[slot, strip(part)]
+        return remote(here, here, r.rows_send.at[index, part], r.rows_recv.at[slot, part], partner)
+
+    def forward(slot, index, partner):
+        for part in range(per_share):
+            passing(slot, index, partner, part).start()
+
+    def arrive(slot):
+        for part in range(per_share):
+            passing(slot, 0, near, part).wait_recv()
+
+    for part in range(per_share):
+        near_mix(0, part).wait_recv()
+        across_mix(part).wait_recv()
+        lax.fori_loop(part * BLOCK // tile, (part + 1) * BLOCK // tile, norms, 0)
+        for index, partner in enumerate((upright, across, near)):
+            passing(mine_at, index, partner, part).start()
     start_line(z == 0, *outward[1][1:])
     to_line(2, mate).start()
     for m, target in outward[2][1:]:
         to_line(m, target).start()
-    pumps(4, 6)
+    start_line(first_z > 0, outward[2][0])
+    pumps(2, 6)
 
     def complete(m):
         own_load(m).wait()
@@ -601,6 +628,11 @@
 
     complete(0)
 
+    def masked(hidden):
+        column = lax.broadcasted_iota(jnp.int32, hidden.shape, 1)
+        held = wide - (z + c) % 2 * extra
+        return jnp.where(column < held, hidden, 0.0).astype(BF16)
+
     def open_gate(slot, at):
         gate = jnp.dot(r.rows[slot], r.gate_all[...], preferred_element_type=F32)
         r.hidden[at] = silu(gate).astype(BF16)
@@ -609,19 +641,21 @@
         d_one, d_two = j % 2, j // 2
         slot = place(c, d_one, d_two)
 
-        @pl.when(j > 0)
-        def _():
-            passing(slot, 0, near).wait_recv()
-            passing(slot, 3 + j, near).start()
-
         @pl.when(j == 1)
         def _():
-            passing(slot, 3, across).start()
-            start_line(first_z > 0, outward[2][0])
+            for part in range(per_share):
+                passing(slot, 0, near, part).wait_recv()
+                passing(slot, 3, across, part).start()
+            forward(slot, 4, near)
+
+        @pl.when(j > 1)
+        def _():
+            arrive(slot)
+            forward(slot, 3 + j, near)
 
         open_gate(slot, kept_at(c, j))
         slot = place(1 - c, d_one, d_two)
-        passing(slot, 0, near).wait_recv()
+        arrive(slot)
         open_gate(slot, 4 + kept_at(1 - c, j))
         return 0
 
@@ -632,17 +666,22 @@
         for core, first in ((c, 0), (1 - c, 4)):
             at = first + kept_at(core, j)
             up = jnp.dot(r.rows[place(core, j % 2, j // 2)], r.up_all[...], preferred_element_type=F32)
-            hidden = r.hidden[at].astype(F32) * up
-            column = lax.broadcasted_iota(jnp.int32, hidden.shape, 1)
-            held = wide - (z + c) % 2 * extra
-            r.hidden[at] = jnp.where(column < held, hidden, 0.0).astype(BF16)
+            r.hidden[at] = masked(r.hidden[at].astype(F32) * up)
         return 0
 
     lax.fori_loop(0, 3, expand, 0)
     start_line(first_z == 0, outward[2][0])
     pump(2, mate)
-    lax.fori_loop(3, 4, gates, 0)
-    lax.fori_loop(3, 4, expand, 0)
+    for part in range(per_share):
+        for core, at in ((c, 3), (1 - c, 7)):
+            slot = place(core, 1, 1)
+            passing(slot, 0, near, part).wait_recv()
+            if at == 3:
+                passing(slot, 6, near, part).start()
+            values = r.rows[slot, strip(part)]
+            gate = jnp.dot(values, r.gate_all[...], preferred_element_type=F32)
+            up = jnp.dot(values, r.up_all[...], preferred_element_type=F32)
+            r.hidden[at, strip(part)] = masked(silu(gate) * up)
 
     chunk = r.got_one.shape[-1]
     per_chunk = chunk // rows
@@ -681,6 +720,22 @@
         pump_chunk(k)
 
     def reduce_step(k, _):
+        @pl.when((k >= 1) & (k < chunks + 1))
+        def _():
+            p = k - 1
+            near_copy(p).wait_recv()
+
+            @pl.when(p >= RING)
+            def _():
+                two_copy(p).wait_send()
+
+            for index, j in enumerate((3, 2)):
+                total = r.mix_local[local_at(p, j)] + r.from_core[p, j].astype(F32)
+                r.hop_two[p % RING, index] = total.astype(BF16)
+            two_copy(p).start()
+            for j in range(2):
+                r.mix_local[local_at(p, j)] = r.mix_local[local_at(p, j)] + r.from_core[p, j].astype(F32)
+
         @pl.when(k < chunks)
         def _():
             for index in range(per_chunk):
@@ -706,22 +761,6 @@
                     r.hidden[j], weights, (((1,), (1,)), ((), ())), preferred_element_type=F32
                 )
 
-        @pl.when((k >= 1) & (k < chunks + 1))
-        def _():
-            p = k - 1
-            near_copy(p).wait_recv()
-
-            @pl.when(p >= RING)
-            def _():
-                two_copy(p).wait_send()
-
-            for index, j in enumerate((3, 2)):
-                total = r.mix_local[local_at(p, j)] + r.from_core[p, j].astype(F32)
-                r.hop_two[p % RING, index] = total.astype(BF16)
-            two_copy(p).start()
-            for j in range(2):
-                r.mix_local[local_at(p, j)] = r.mix_local[local_at(p, j)] + r.from_core[p, j].astype(F32)
-
         @pl.when((k >= 2) & (k < chunks + 2))
         def _():
             p = k - 2
@@ -775,11 +814,12 @@
             to_line(m, target).wait_send()
         for source in range(count):
             relay(m, source).wait_send()
-    near_mix(0).wait_send()
-    near_mix(1).wait_send()
-    across_mix.wait_send()
-    for index in range(7):
-        passing(mine_at, index, near).wait_send()
+    for part in range(per_share):
+        near_mix(0, part).wait_send()
+        near_mix(1, part).wait_send()
+        across_mix(part).wait_send()
+        for index in range(7):
+            passing(mine_at, index, near, part).wait_send()
     for slot in range(min(RING, chunks)):
         near_copy(slot).wait_send()
         two_copy(slot).wait_send()
@@ -921,10 +961,10 @@
         "state_recv": dma((1,)),
         "line_send": dma((hops,)),
         "line_recv": dma((hops,)),
-        "mix_send": dma((3,)),
-        "mix_recv": dma((3,)),
-        "rows_send": dma((7,)),
-        "rows_recv": dma((8,)),
+        "mix_send": dma((3, share // BLOCK)),
+        "mix_recv": dma((3, share // BLOCK)),
+        "rows_send": dma((7, share // BLOCK)),
+        "rows_recv": dma((8, share // BLOCK)),
         "core_send": dma((RING,)),
         "core_recv": dma((chunks,)),
         "two_send": dma((RING,)),

time: 178 us -> 170 us (0.955)
  Pallas kernels: 170 us -> 160 us
    pallas_call x1, Pallas kernels: 170 us -> 160 us  [layer(): pl.pallas_call(functools.partial(layer_kernel, names, sizes, columns - wi...]
where the time goes in v4:
time: 170 us; the launch traced here: 167 us
  Pallas kernels  160 us (94%)
  local copies, waits for them, and re-layouts  5.72 us (3%)
    pallas_call x1, Pallas kernels, layer(): pl.pallas_call(functools.partial(layer_kernel, names, sizes, columns - wi...  160 us

profile of v4, /device:TPU:24, one launch (start us, length us, event | category | flops | bytes accessed | tf_op | source)
XLA Modules:
  0.0 166.7 jit_solution(12700161939637324695)
XLA Ops:
  0.0 0.7 pad_maximum_fusion
  0.7 0.2 copy.28
  1.0 0.9 pad.4.refs_12_
  1.8 2.3 %copy_bitcast_fusion = (bf16[1024,256]{1,0:T(8,128)(2,1)}, bf16[1024,256]{1,0:T(8,128)(2,1)}) fusion(bf16[128,8,2,128]{3,2,1,0:T(2,128)(2,1)} %bitcast.6, bf16[128,8,2,128]{3,2,1,0:T(2,128)(2,1)} %bitcast.7), kind=kLoop, calls=%fused_computation | loop fusion | bytes 2097152 | tf_op jit(solution)/shard_map/reshape | solution.py:859
  4.2 160.2 %layer.1 = bf16[256,2048]{1,0:T(8,128)(2,1)} custom-call(bf16[1024,256]{1,0:T(8,128)(2,1)} %refs_0_.1, bf16[1024,256]{1,0:T(8,128)(2,1)} %refs_1_.1, bf16[1024,256]{1,0:T(8,128)(2,1)} %get-tuple-element.6.refs_2_, bf16[1024,256]{1,0:T(8,128)(2,1)} %get-tuple-element.5.refs_3_, bf16[1024,256]{1,0:T(8,128)(2,1)} %refs_4_.1, bf16[1024,256]{1,0:T(8,128)(2,1)} %refs_5_.1, ...), custom_call_target="tpu_custom_call" | custom-call | flops 40000000000 | bytes 524288 | tf_op jit(solution)/shard_map/layer/pallas_call | solution.py:976
  164.4 2.3 %copy.34 = bf16[256,2048]{1,0:T(8,128)(2,1)} copy(bf16[256,2048]{1,0:T(8,128)(2,1)} %layer.1) | data formatting | bytes 2097152
